TPU v7x, 256 devices: a whole 4x4x8 slice. The times are simulated.
256 devices in a mesh: ep: 64 (over z, x, core), tp: 4 (over y).
Axes of the slice: x: 4, y: 4, z: 8, core: 2. Of those that a mesh axis runs over, the one named last changes fastest.
Arguments:
- mixer_input: bfloat16 [40960, 2048], P('ep'), may hold values from -6 to 6
- mixer_gain: float32 [2048], replicated, may hold values from 0.1 to 1.9
- value_weight: bfloat16 [2048, 1024], P(None, 'tp'), may hold values from -0.125 to 0.125
- inner_gate: bfloat16 [2048, 1024], P(None, 'tp'), may hold values from -0.125 to 0.125
- outer_gate: bfloat16 [2048, 1024], P(None, 'tp'), may hold values from -0.125 to 0.125
- kernel_taps: float32 [3, 1024], P(None, 'tp'), may hold values from -3 to 3
- mixer_proj: bfloat16 [1024, 2048], P('tp'), may hold values from -0.1875 to 0.1875
- expert_input: bfloat16 [40960, 2048], P(('ep', 'tp')), may hold values from -6 to 6
- expert_gain: float32 [2048], replicated, may hold values from 0.1 to 1.9
- routes: int32 [40960, 2], P(('ep', 'tp')), may hold values from 0 to 63, as said below
- group_logits: float32 [40960, 8], P(('ep', 'tp')), may hold values from -6 to 6
- pair_logits: float32 [40960, 2], P(('ep', 'tp')), may hold values from -6 to 6
- gate_weight: bfloat16 [64, 2048, 1024], P('ep', None, 'tp'), may hold values from -0.125 to 0.125
- up_weight: bfloat16 [64, 2048, 1024], P('ep', None, 'tp'), may hold values from -0.125 to 0.125
- down_weight: bfloat16 [64, 1024, 2048], P('ep', 'tp'), may hold values from -0.75 to 0.75
Outputs:
- mixer_output: bfloat16 [40960, 2048], P(('ep', 'tp'))
- expert_output: bfloat16 [40960, 2048], P(('ep', 'tp'))
Inputs may be any that keep to these rules, and one draw needn't show every extreme that they name: `routes`: both entries of a row are different experts of one group (equal after integer division by 8). In the rows of one device every group is chosen by the same number of rows, no expert is named more than 10 times, and in every draw one expert is named exactly 10 times in the rows of every device.
All inputs are finite; a program needn't handle non-finite values.
Results may differ from a plain program's by a relative error of at most 0.01.
Values may be sent and summed in bfloat16 or wider, within the bound.
A program may use at most 128 MiB of HBM per device.

v0:
```python
import jax
import jax.numpy as jnp
from jax import lax
from jax.sharding import PartitionSpec as P

EPG = 8


EPSILON = 1e-06


def padded_2(cells, sides, width):
    for axis, dim in sides:
        count = lax.axis_size(axis)
        ends = count - 1
        head = lax.slice_in_dim(cells, 0, width, axis=dim)
        tail = lax.slice_in_dim(cells, cells.shape[dim] - width, cells.shape[dim], axis=dim)
        cells = jnp.concatenate(
            [
                lax.ppermute(tail, axis, [(i, (i + 1) % count) for i in range(ends)]),
                cells,
                lax.ppermute(head, axis, [((i + 1) % count, i) for i in range(ends)]),
            ],
            axis=dim,
        )
    return cells


def split_up(x, dim, length):
    shape = x.shape
    blocks = x.reshape(*shape[:dim], length, shape[dim] // length, *shape[dim + 1 :])
    return jnp.moveaxis(blocks, dim, 0)


def sent_and_summed(x, axis, dim):
    length = lax.axis_size(axis)
    blocks = lax.all_to_all(split_up(x, dim, length), axis, 0, 0, tiled=True)
    return jnp.sum(blocks.astype(jnp.float32), axis=0)


def turned_gather(arrays, axis, dims):
    turned = [jnp.moveaxis(a, dim, 0) for a, dim in zip(arrays, dims)]
    widths = [t[0].size for t in turned]
    both = jnp.concatenate([t.reshape(-1, w) for t, w in zip(turned, widths)], axis=1)
    result = lax.all_gather(both, axis, axis=0, tiled=True)
    blocks = jnp.split(result, [sum(widths[:k]) for k in range(1, len(widths))], axis=1)
    return tuple(
        (
            jnp.moveaxis(b.reshape(-1, *t.shape[1:]), 0, dim)
            for b, t, dim in zip(blocks, turned, dims)
        )
    )


def normed(values, gain):
    wide = values.astype(jnp.float32)
    scale = lax.rsqrt(jnp.mean(wide * wide, axis=-1, keepdims=True) + EPSILON)
    return (wide * scale * gain).astype(jnp.bfloat16)


def blockwise_sum(left, right, blocks):
    width = left.shape[1] // blocks
    total = jnp.zeros((left.shape[0], right.shape[1]), jnp.float32)
    for block in range(blocks):
        part = jnp.dot(
            left[:, block * width : (block + 1) * width],
            right[block * width : (block + 1) * width],
            preferred_element_type=jnp.float32,
        )
        rounded = lax.optimization_barrier(part.astype(jnp.bfloat16))
        total = total + rounded.astype(jnp.float32)
    return total.astype(jnp.bfloat16)


def route_weights(routes, group_logits, pair_logits):
    chosen = routes[:, 0] // EPG
    groups = jnp.arange(group_logits.shape[1], dtype=jnp.int32)
    picked = jnp.sum(jnp.where(groups[None, :] == chosen[:, None], group_logits, 0.0), axis=1)
    group_weight = 1.0 / jnp.sum(jnp.exp(group_logits - picked[:, None]), axis=1)
    return group_weight[:, None] * jax.nn.sigmoid(pair_logits - pair_logits[:, ::-1])


def on_device(
    mixer_input,
    mixer_gain,
    value_weight,
    inner_gate,
    outer_gate,
    kernel_taps,
    mixer_proj,
    expert_input,
    expert_gain,
    routes,
    group_logits,
    pair_logits,
    gate_weight,
    up_weight,
    down_weight,
):
    split = lax.axis_size("tp")
    normal_rows = normed(mixer_input, mixer_gain)
    values = jnp.dot(normal_rows, value_weight, preferred_element_type=jnp.float32)
    inner = jnp.dot(normal_rows, inner_gate, preferred_element_type=jnp.float32)
    outer = jnp.dot(normal_rows, outer_gate, preferred_element_type=jnp.float32)
    mixed_in = (inner * values).astype(jnp.bfloat16)
    padded = padded_2(mixed_in, (("ep", 0),), 1).astype(jnp.float32)
    conv_sum = (
        kernel_taps[0] * padded[:-2] + kernel_taps[1] * padded[1:-1] + kernel_taps[2] * padded[2:]
    )
    mixer_rows = (outer * conv_sum).astype(jnp.bfloat16)
    mixer_output = sent_and_summed(
        jnp.dot(mixer_rows, mixer_proj, preferred_element_type=jnp.float32).astype(jnp.bfloat16),
        "tp",
        0,
    ).astype(jnp.bfloat16)
    expert_norm = normed(expert_input, expert_gain)
    weights = route_weights(routes, group_logits, pair_logits)
    experts = lax.axis_size("ep")
    local = expert_norm.shape[0]
    width = expert_norm.shape[1]
    capacity = 4 * local // experts
    flat = routes.reshape(-1)
    onehot = (flat[:, None] == jnp.arange(experts, dtype=jnp.int32)[None, :]).astype(jnp.int32)
    before = jnp.sum((jnp.cumsum(onehot, axis=0) - onehot) * onehot, axis=1)
    slots = flat * capacity + before
    sources = (
        jnp.full((experts * capacity,), local, jnp.int32)
        .at[slots]
        .set(jnp.arange(2 * local, dtype=jnp.int32) // 2)
    )
    rows_pad = jnp.concatenate([expert_norm, jnp.zeros((1, width), jnp.bfloat16)])
    outgoing = rows_pad[sources].reshape(experts, capacity, width)
    whole_gate, whole_up, whole_down = turned_gather(
        (gate_weight, up_weight, down_weight), "tp", (2, 2, 1)
    )
    arrived = lax.all_to_all(outgoing, "ep", split_axis=0, concat_axis=0, tiled=True)
    senders, items, _ = arrived.shape
    answers = expert_block_local(
        arrived.reshape(senders * items, width), whole_gate[0], whole_up[0], whole_down[0], split
    )
    returned = lax.all_to_all(
        answers.reshape(senders, items, width), "ep", split_axis=0, concat_axis=0, tiled=True
    )
    answered = returned.reshape(experts * capacity, width)
    pairs = answered[slots].reshape(local, 2, width)
    expert_output = (
        weights[:, 0:1] * pairs[:, 0].astype(jnp.float32)
        + weights[:, 1:2] * pairs[:, 1].astype(jnp.float32)
    ).astype(jnp.bfloat16)
    return (mixer_output, expert_output)


def expert_block_local(rows, gate, upper, down, blocks):
    first = jnp.dot(rows, gate, preferred_element_type=jnp.float32)
    second = jnp.dot(rows, upper, preferred_element_type=jnp.float32)
    hidden = (jax.nn.silu(first) * second).astype(jnp.bfloat16)
    return blockwise_sum(hidden, down, blocks)


def solution(mesh):
    in_specs = (
        P("ep", None),
        P(),
        P(None, "tp"),
        P(None, "tp"),
        P(None, "tp"),
        P(None, "tp"),
        P("tp", None),
        P(("ep", "tp"), None),
        P(),
        P(("ep", "tp"), None),
        P(("ep", "tp"), None),
        P(("ep", "tp"), None),
        P("ep", None, "tp"),
        P("ep", None, "tp"),
        P("ep", "tp", None),
    )
    out_specs = (P(("ep", "tp"), None), P(("ep", "tp"), None))
    return jax.shard_map(
        on_device, mesh=mesh, in_specs=in_specs, out_specs=out_specs, check_vma=False
    )
```

profile of v0, /device:TPU:8, one launch (start us, length us, event | category | flops | bytes accessed | tf_op | source)
XLA Modules:
  0.0 300.3 jit_solution(1046094954422467291)
XLA Ops:
  7.2 1.6 copy.26
  8.8 1.5 copy.25
  10.3 2.9 pad_maximum_fusion
  13.2 0.7 copy-done.7
  13.8 0.1 copy.22
  13.9 0.1 eq.41
  14.1 0.9 reduce-window.6
  15.0 0.2 slice_reduce_fusion
  15.3 0.1 copy.21
  15.4 0.1 mul.155
  15.6 0.2 fusion.5
  15.8 0.2 fusion.7
  16.0 0.1 concatenate.10
  16.1 0.1 bitcast_bitcast_fusion
  16.3 2.9 scatter_custom_fusion
  19.2 4.2 %gather_fusion = bf16[640,2048]{1,0:T(8,128)(2,1)} fusion(bf16[161,2048]{1,0:T(8,128)(2,1)S(1)} %concatenate.10, s32[1024]{0:T(1024)S(1)} %pad_clamp_fusion.1), kind=kCustom, calls=%fused_computation | custom fusion | bytes 5245440 | tf_op jit(solution)/shard_map/gather | solution.py:132
  23.4 5.4 %reshape.104 = bf16[64,10,2048]{2,1,0:T(8,128)(2,1)} reshape(bf16[640,2048]{1,0:T(8,128)(2,1)} %gather_fusion) | data formatting | bytes 5242880 | tf_op jit(solution)/shard_map/reshape | solution.py:132
  28.8 12.4 %all-to-all-start.1 = ((bf16[64,10,2048]{2,1,0:T(8,128)(2,1)}), bf16[64,10,2048]{2,1,0:T(8,128)(2,1)}, u32[]{:S(2)}, u32[]{:S(2)}) async-start(bf16[64,10,2048]{2,1,0:T(8,128)(2,1)} %reshape.104), calls=%async_computation.1 | async-start | bytes 8388608 | tf_op jit(solution)/shard_map/all_to_all | solution.py:136
  41.3 2.5 fusion
  43.8 0.9 fusion.36
  44.7 0.3 copy-done.12
  45.0 0.9 fusion.11
  46.0 1.9 collective-permute-start
  47.9 1.3 collective-permute-start.1
  49.2 2.8 collective-permute-done.1
  52.1 0.1 maximum_convert_fusion
  52.1 6.5 %convolution_convert_fusion.4 = bf16[640,2048]{1,0:T(8,128)(2,1)} fusion(bf16[256,2048]{1,0:T(8,128)(2,1)S(1)} %copy-done, bf16[2048,256]{1,0:T(8,128)(2,1)} %param.19, f32[642,256]{1,0:T(8,128)S(1)} %maximum_convert_fusion, f32[256]{0:T(256)S(1)} %bitcast.68, f32[256]{0:T(256)S(1)} %bitcast.69, f32[256]{0:T(256)S(1)} %bitcast.67, ...), kind=kOutput, calls=%fused_computation.17 | convolution fusion | flops 1349877760 | bytes 9321472 | tf_op jit(solution)/shard_map/dot_general | solution.py:112
  58.6 78.9 %all-to-all-done.1 = bf16[64,10,2048]{2,1,0:T(8,128)(2,1)} async-done(((bf16[64,10,2048]{2,1,0:T(8,128)(2,1)}), bf16[64,10,2048]{2,1,0:T(8,128)(2,1)}, u32[]{:S(2)}, u32[]{:S(2)}) %all-to-all-start.1) | async-done | bytes 2621472 | tf_op jit(solution)/shard_map/all_to_all | solution.py:136
  137.5 4.9 %all-to-all-start = ((bf16[4,160,2048]{2,1,0:T(8,128)(2,1)}), bf16[4,160,2048]{2,1,0:T(8,128)(2,1)S(1)}, u32[]{:S(2)}, u32[]{:S(2)}) async-start(bf16[4,160,2048]{2,1,0:T(8,128)(2,1)} %bitcast.61), calls=%async_computation | async-start | bytes 5242880 | tf_op jit(solution)/shard_map/all_to_all | solution.py:37
  142.4 5.5 %reshape.105 = bf16[640,2048]{1,0:T(8,128)(2,1)} reshape(bf16[64,10,2048]{2,1,0:T(8,128)(2,1)} %all-to-all-done.1) | data formatting | bytes 5242880 | tf_op jit(solution)/shard_map/reshape | solution.py:139
  147.9 5.7 %fusion.4 = f32[640,1024]{1,0:T(8,128)S(1)} fusion(bf16[640,2048]{1,0:T(8,128)(2,1)} %reshape.105, bf16[1024,6144]{1,0:T(8,128)(2,1)} %all-gather.2.cloned.1.call-done), kind=kOutput, calls=%fused_computation.12 | convolution fusion | flops 2684354560 | bytes 9437184 | tf_op jit(solution)/shard_map/dot_general | solution.py:154
  153.6 1.7 copy-done.5
  155.3 3.1 %multiply_convert_fusion = bf16[640,1024]{1,0:T(8,128)(2,1)S(1)} fusion(f32[640,1024]{1,0:T(8,128)S(1)} %fusion.4, bf16[640,2048]{1,0:T(8,128)(2,1)S(1)} %copy-done.3, bf16[1024,6144]{1,0:T(8,128)(2,1)S(1)} %copy-done.5), kind=kOutput, calls=%fused_computation.19 | convolution fusion | flops 2688286720 | bytes 10747904 | tf_op jit(solution)/shard_map/dot_general | solution.py:155
  158.4 0.8 convolution_convert_fusion.3
  159.3 0.9 convolution_convert_fusion.2
  160.2 0.9 convolution_convert_fusion.1
  161.0 2.1 convolution_convert_fusion
  163.1 3.9 %add_convert_fusion = bf16[640,2048]{1,0:T(8,128)(2,1)} fusion(bf16[640,2048]{1,0:T(8,128)(2,1)S(1)} %convolution_convert_fusion, bf16[640,2048]{1,0:T(8,128)(2,1)S(1)} %convolution_convert_fusion.1, bf16[640,2048]{1,0:T(8,128)(2,1)S(1)} %convolution_convert_fusion.2, bf16[640,2048]{1,0:T(8,128)(2,1)S(1)} %convolution_convert_fusion.3), kind=kLoop, calls=%fused_computation.8 | loop fusion | flops 10485760 | bytes 13107200 | tf_op jit(solution)/shard_map/convert_element_type | solution.py:72
  167.0 5.4 %reshape.110 = bf16[64,10,2048]{2,1,0:T(8,128)(2,1)} reshape(bf16[640,2048]{1,0:T(8,128)(2,1)} %add_convert_fusion) | data formatting | bytes 5242880 | tf_op jit(solution)/shard_map/reshape | solution.py:142
  172.4 10.8 %all-to-all-start.2 = ((bf16[64,10,2048]{2,1,0:T(8,128)(2,1)}), bf16[64,10,2048]{2,1,0:T(8,128)(2,1)}, u32[]{:S(2)}, u32[]{:S(2)}) async-start(bf16[64,10,2048]{2,1,0:T(8,128)(2,1)} %reshape.110), calls=%async_computation.2 | async-start | bytes 8388608 | tf_op jit(solution)/shard_map/all_to_all | solution.py:141
  183.2 0.1 rev.3
  183.4 1.5 reduce_sum.60
  184.9 94.3 %all-to-all-done.2 = bf16[64,10,2048]{2,1,0:T(8,128)(2,1)} async-done(((bf16[64,10,2048]{2,1,0:T(8,128)(2,1)}), bf16[64,10,2048]{2,1,0:T(8,128)(2,1)}, u32[]{:S(2)}, u32[]{:S(2)}) %all-to-all-start.2) | async-done | bytes 2621472 | tf_op jit(solution)/shard_map/all_to_all | solution.py:141
  279.2 4.1 %reshape.111 = bf16[640,2048]{1,0:T(8,128)(2,1)S(1)} reshape(bf16[64,10,2048]{2,1,0:T(8,128)(2,1)} %all-to-all-done.2) | data formatting | bytes 5242880 | tf_op jit(solution)/shard_map/reshape | solution.py:144
  283.3 3.0 %gather_fusion.1 = bf16[320,2048]{1,0:T(8,128)(2,1)} fusion(bf16[640,2048]{1,0:T(8,128)(2,1)S(1)} %reshape.111, s32[1024]{0:T(1024)S(1)} %pad_clamp_fusion), kind=kCustom, calls=%fused_computation.1 | custom fusion | bytes 2622720 | tf_op jit(solution)/shard_map/gather | solution.py:145
  286.3 3.1 %reshape.112 = bf16[160,2,2048]{2,1,0:T(2,128)(2,1)S(1)} reshape(bf16[320,2048]{1,0:T(8,128)(2,1)} %gather_fusion.1) | data formatting | bytes 2621440 | tf_op jit(solution)/shard_map/reshape | solution.py:145
  289.4 1.8 fusion.40
  291.3 2.2 fusion.9
  (50 shorter events, 0.4 us)
Async XLA Ops:
  7.2 45.0 %copy-start = (bf16[256,2048]{1,0:T(8,128)(2,1)S(1)}, bf16[256,2048]{1,0:T(8,128)(2,1)}, u32[]{:S(2)}) copy-start(bf16[256,2048]{1,0:T(8,128)(2,1)} %param.21) | copy-start | bytes 3145732
  7.2 140.7 %all-gather.2.cloned.1.call-start = ((), (), s32[]{:S(2)}) async-start(), calls=%async_computation.3 | async-start | bytes 15728640 | tf_op jit(solution)/shard_map/all_gather | solution.py:45
  13.1 0.7 copy-start.7
  13.1 2.4 copy-start.4
  13.1 2.7 copy-start.8
  28.8 14.9 %copy-start.11 = (bf16[2048,256]{1,0:T(8,128)(2,1)S(1)}, bf16[2048,256]{1,0:T(8,128)(2,1)}, u32[]{:S(2)}) copy-start(bf16[2048,256]{1,0:T(8,128)(2,1)} %param.18) | copy-start | bytes 3145732
  28.8 108.6 %all-to-all-start.1 = ((bf16[64,10,2048]{2,1,0:T(8,128)(2,1)}), bf16[64,10,2048]{2,1,0:T(8,128)(2,1)}, u32[]{:S(2)}, u32[]{:S(2)}) async-start(bf16[64,10,2048]{2,1,0:T(8,128)(2,1)} %reshape.104), calls=%async_computation.1 | async-start | bytes 8388608 | tf_op jit(solution)/shard_map/all_to_all | solution.py:136
  41.2 2.5 copy-start.2
  41.2 2.5 copy-start.13
  43.8 1.2 copy-start.12
  45.0 4.2 %copy-start.10 = (f32[3,256]{1,0:T(4,128)S(1)}, f32[3,256]{1,0:T(4,128)}, u32[]{:S(2)}) copy-start(f32[3,256]{1,0:T(4,128)} %param.20) | copy-start | bytes 9220
  46.0 3.3 %collective-permute-start = (bf16[1,256]{1,0:T(2,128)(2,1)S(1)}, bf16[1,256]{1,0:T(2,128)(2,1)S(1)}, u32[]{:S(2)}, u32[]{:S(2)}) collective-permute-start(bf16[1,256]{1,0:T(2,128)(2,1)S(1)} %get-tuple-element.4), channel_id=1, source_target_pairs={{0,4},{4,8},{8,12},{12,16},{16,20},{20,24},{24,28},{28,32},{32,36}... | collective-permute-start | bytes 1544 | tf_op jit(solution)/shard_map/ppermute | solution.py:20
  47.9 4.2 %collective-permute-start.1 = (bf16[1,256]{1,0:T(2,128)(2,1)S(1)}, bf16[1,256]{1,0:T(2,128)(2,1)S(1)}, u32[]{:S(2)}, u32[]{:S(2)}) collective-permute-start(bf16[1,256]{1,0:T(2,128)(2,1)S(1)} %get-tuple-element.5), channel_id=1, source_target_pairs={{4,0},{8,4},{12,8},{16,12},{20,16},{24,20},{28,24},{32,28},{36,32}... | collective-permute-start | bytes 1544 | tf_op jit(solution)/shard_map/ppermute | solution.py:22
  137.5 34.9 %all-to-all-start = ((bf16[4,160,2048]{2,1,0:T(8,128)(2,1)}), bf16[4,160,2048]{2,1,0:T(8,128)(2,1)S(1)}, u32[]{:S(2)}, u32[]{:S(2)}) async-start(bf16[4,160,2048]{2,1,0:T(8,128)(2,1)} %bitcast.61), calls=%async_computation | async-start | bytes 5242880 | tf_op jit(solution)/shard_map/all_to_all | solution.py:37
  147.9 5.7 %copy-start.3 = (bf16[640,2048]{1,0:T(8,128)(2,1)S(1)}, bf16[640,2048]{1,0:T(8,128)(2,1)}, u32[]{:S(2)}) copy-start(bf16[640,2048]{1,0:T(8,128)(2,1)} %reshape.105) | copy-start | bytes 7864324
  147.9 7.4 %copy-start.5 = (bf16[1024,6144]{1,0:T(8,128)(2,1)S(1)}, bf16[1024,6144]{1,0:T(8,128)(2,1)}, u32[]{:S(2)}) copy-start(bf16[1024,6144]{1,0:T(8,128)(2,1)} %all-gather.2.cloned.1.call-done) | copy-start | bytes 37748740
  172.4 10.8 %copy-start.9 = (f32[160,2]{0,1:T(2,128)S(1)}, f32[160,2]{0,1:T(2,128)}, u32[]{:S(2)}) copy-start(f32[160,2]{0,1:T(2,128)} %param.26) | copy-start | bytes 3844
  172.4 10.9 %copy-start.6 = (f32[160,8]{0,1:T(8,128)S(1)}, f32[160,8]{0,1:T(8,128)}, u32[]{:S(2)}) copy-start(f32[160,8]{0,1:T(8,128)} %param.25) | copy-start | bytes 15364
  172.4 106.8 %all-to-all-start.2 = ((bf16[64,10,2048]{2,1,0:T(8,128)(2,1)}), bf16[64,10,2048]{2,1,0:T(8,128)(2,1)}, u32[]{:S(2)}, u32[]{:S(2)}) async-start(bf16[64,10,2048]{2,1,0:T(8,128)(2,1)} %reshape.110), calls=%async_computation.2 | async-start | bytes 8388608 | tf_op jit(solution)/shard_map/all_to_all | solution.py:141
  289.4 4.0 %copy-start.1 = (bf16[256,2048]{1,0:T(8,128)(2,1)S(1)}, bf16[256,2048]{1,0:T(8,128)(2,1)}, u32[]{:S(2)}) copy-start(bf16[256,2048]{1,0:T(8,128)(2,1)} %param.21) | copy-start | bytes 3145732
Sparse Core Ops, SparseCore 0:
  13.3 123.9 all-gather.1
where the time goes:
time: 301 us; the launch traced here: 300 us
  waiting for transfers between devices  176 us (58%)
  local copies, waits for them, and re-layouts  42.1 us (14%)
  starting transfers between devices  31.3 us (10%)
  matrix products  21.8 us (7%)
  other arithmetic  14.6 us (5%)
  between operations  14.4 us (5%)
    all_to_all x1, waiting for transfers between devices, on_device(): lax.all_to_all(answers.reshape(senders, items, width), 'ep', split_axis=0...  94.3 us
    all_to_all x1, waiting for transfers between devices, on_device(): lax.all_to_all(outgoing, 'ep', split_axis=0, concat_axis=0, tiled=True)  78.9 us
    all_to_all x1, starting transfers between devices, on_device(): lax.all_to_all(outgoing, 'ep', split_axis=0, concat_axis=0, tiled=True)  12.4 us
    all_to_all x1, starting transfers between devices, on_device(): lax.all_to_all(answers.reshape(senders, items, width), 'ep', split_axis=0...  10.8 us
    dot_general x1, matrix products, on_device(): jnp.dot(mixer_rows, mixer_proj, preferred_element_type=jnp.float32)  6.46 us
  transfers between devices with their start and end apart: 6, of which 3 were waited for; matrix products, arithmetic and copies ran while one was open for 19% of the time, Pallas kernels for 0%

commit v1 on v0

v1 whole, which is shorter than its diff:
```python
import jax
import jax.numpy as jnp
from jax import lax
from jax.sharding import PartitionSpec as P

EPG = 8
EPSILON = 1e-06


def padded_2(cells, axis):
    count = lax.axis_size(axis)
    ends = count - 1
    head = cells[:1]
    tail = cells[-1:]
    return jnp.concatenate(
        [
            lax.ppermute(tail, axis, [(i, i + 1) for i in range(ends)]),
            cells,
            lax.ppermute(head, axis, [(i + 1, i) for i in range(ends)]),
        ],
        axis=0,
    )


def normed(values, gain):
    wide = values.astype(jnp.float32)
    scale = lax.rsqrt(jnp.mean(wide * wide, axis=-1, keepdims=True) + EPSILON)
    return (wide * scale * gain).astype(jnp.bfloat16)


def route_weights(routes, group_logits, pair_logits):
    chosen = routes[:, 0] // EPG
    groups = jnp.arange(group_logits.shape[1], dtype=jnp.int32)
    picked = jnp.sum(jnp.where(groups[None, :] == chosen[:, None], group_logits, 0.0), axis=1)
    group_weight = 1.0 / jnp.sum(jnp.exp(group_logits - picked[:, None]), axis=1)
    return group_weight[:, None] * jax.nn.sigmoid(pair_logits - pair_logits[:, ::-1])


def f32dot(a, b):
    return jnp.dot(a, b, preferred_element_type=jnp.float32)


def on_device(
    mixer_input, mixer_gain, value_weight, inner_gate, outer_gate, kernel_taps, mixer_proj,
    expert_input, expert_gain, routes, group_logits, pair_logits, gate_weight, up_weight, down_weight,
):
    split = lax.axis_size("tp")
    experts = lax.axis_size("ep")
    n_groups = experts // EPG
    local = expert_input.shape[0]
    width = expert_input.shape[1]
    per = local // n_groups
    expert_norm = normed(expert_input, expert_gain)
    weights = route_weights(routes, group_logits, pair_logits)
    member = routes % EPG
    lanes = jnp.arange(EPG, dtype=jnp.int32)
    wide_w = (
        jnp.where(member[:, 0:1] == lanes, weights[:, 0:1], 0.0)
        + jnp.where(member[:, 1:2] == lanes, weights[:, 1:2], 0.0)
    )
    high = wide_w.astype(jnp.bfloat16)
    low = (wide_w - high.astype(jnp.float32)).astype(jnp.bfloat16)
    extra = jnp.concatenate([high, low, jnp.zeros((local, 128 - 2 * EPG), jnp.bfloat16)], axis=1)
    group = routes[:, 0] // EPG
    place = jnp.arange(local, dtype=jnp.int32)
    earlier = (group[:, None] == group[None, :]) & (place[None, :] < place[:, None])
    slot = group * per + jnp.sum(earlier.astype(jnp.int32), axis=1)
    onehot = (slot[:, None] == place[None, :]).astype(jnp.bfloat16)
    rows = jnp.concatenate([expert_norm, extra], axis=1)
    ordered = lax.dot_general(
        onehot, rows, (((0,), (0,)), ((), ())), preferred_element_type=jnp.float32
    ).astype(jnp.bfloat16)
    z_groups = [[z * EPG + i for z in range(n_groups)] for i in range(EPG)]
    plane_groups = [[z * EPG + i for i in range(EPG)] for z in range(n_groups)]
    arrived = lax.all_to_all(
        ordered, "ep", split_axis=0, concat_axis=0, axis_index_groups=z_groups, tiled=True
    )
    everyone = lax.all_gather(
        arrived, "ep", axis=0, axis_index_groups=plane_groups, tiled=True
    )
    all_gate = lax.all_gather(gate_weight[0], "tp", axis=0)
    all_up = lax.all_gather(up_weight[0], "tp", axis=0)
    all_down = lax.all_gather(down_weight[0], "tp", axis=0, tiled=True)

    normal_rows = normed(mixer_input, mixer_gain)
    values = f32dot(normal_rows, value_weight)
    inner = f32dot(normal_rows, inner_gate)
    outer = f32dot(normal_rows, outer_gate)
    mixed_in = (inner * values).astype(jnp.bfloat16)
    padded = padded_2(mixed_in, "ep").astype(jnp.float32)
    conv_sum = (
        kernel_taps[0] * padded[:-2] + kernel_taps[1] * padded[1:-1] + kernel_taps[2] * padded[2:]
    )
    mixer_rows = (outer * conv_sum).astype(jnp.bfloat16)
    partial = f32dot(mixer_rows, mixer_proj).astype(jnp.bfloat16)
    blocks = lax.all_to_all(partial.reshape(split, -1, width), "tp", 0, 0, tiled=True)
    mixer_output = jnp.sum(blocks.astype(jnp.float32), axis=0).astype(jnp.bfloat16)

    tokens = everyone[:, :width]
    mine = lax.axis_index("ep") % EPG
    both = everyone[:, width:].astype(jnp.float32)
    spot = jnp.arange(128, dtype=jnp.int32)
    weight = jnp.sum(jnp.where((spot == mine) | (spot == mine + EPG), both, 0.0), axis=1, keepdims=True)
    parts = []
    for j in range(split):
        first = f32dot(tokens, all_gate[j])
        second = f32dot(tokens, all_up[j])
        parts.append((jax.nn.silu(first) * second).astype(jnp.bfloat16))
    hidden = jnp.concatenate(parts, axis=1)
    answers = (f32dot(hidden, all_down) * weight).astype(jnp.bfloat16)
    home = lax.psum_scatter(
        answers, "ep", scatter_dimension=0, axis_index_groups=plane_groups, tiled=True
    )
    back = lax.all_to_all(
        home, "ep", split_axis=0, concat_axis=0, axis_index_groups=z_groups, tiled=True
    )
    expert_output = f32dot(onehot, back).astype(jnp.bfloat16)
    return (mixer_output, expert_output)


def solution(mesh):
    in_specs = (
        P("ep", None), P(), P(None, "tp"), P(None, "tp"), P(None, "tp"), P(None, "tp"), P("tp", None),
        P(("ep", "tp"), None), P(), P(("ep", "tp"), None), P(("ep", "tp"), None), P(("ep", "tp"), None),
        P("ep", None, "tp"), P("ep", None, "tp"), P("ep", "tp", None),
    )
    out_specs = (P(("ep", "tp"), None), P(("ep", "tp"), None))
    return jax.shard_map(
        on_device, mesh=mesh, in_specs=in_specs, out_specs=out_specs, check_vma=False
    )
```

time: 301 us -> 351 us (1.17)
  waiting for transfers between devices: 176 us -> 214 us
  local copies, waits for them, and re-layouts: 42.1 us -> 5.27 us
  blocking collectives: 0 us -> 32.4 us
  matrix products: 21.8 us -> 50.3 us
  starting transfers between devices: 31.3 us -> 19.4 us
    all_gather x1 -> x4, waiting for transfers between devices: 0.01 us -> 162 us  [the longest x1 50.9 us: on_device(): all_gate = lax.all_gather(gate_weight[0], 'tp', axis=0)]
    all_to_all x3 -> x2, waiting for transfers between devices: 173 us -> 27.4 us  [the longest x1 18.3 us: on_device(): lax.all_to_all(home, 'ep', split_axis=0, concat_axis=0, axis_index_groups...]
    all_to_all x0 -> x1, blocking collectives: none -> 32.4 us  [on_device(): lax.all_to_all(ordered, 'ep', split_axis=0, concat_axis=0, axis_index_gro...]
    dot_general x9 -> x14, matrix products: 21.8 us -> 50.3 us  [the longest x13 49.8 us: f32dot(): return jnp.dot(a, b, preferred_element_type=jnp.float32)]
    reshape x5 -> x0, local copies, waits for them, and re-layouts: 23.5 us -> none  [the longest x1 5.52 us: on_device(): arrived.reshape(senders * items, width)]
    reduce_scatter x0 -> x1, waiting for transfers between devices: none -> 19 us  [on_device(): lax.psum_scatter(answers, 'ep', scatter_dimension=0, axis_index_groups=pl...]
    all_to_all x3 -> x2, starting transfers between devices: 28.1 us -> 16.3 us  [the longest x1 10.7 us: on_device(): lax.all_to_all(home, 'ep', split_axis=0, concat_axis=0, axis_index_groups...]
    gather x2 -> x0, local copies, waits for them, and re-layouts: 7.2 us -> none  [the longest x1 4.16 us: on_device(): outgoing = rows_pad[sources].reshape(experts, capacity, width)]
  transfers between devices with their start and end apart: 6 -> 9, of which waited for: 3 -> 8; matrix products, arithmetic and copies ran while one was open for 19% -> 13% of each run, Pallas kernels for 0% -> 0%
where the time goes in v1:
time: 351 us; the launch traced here: 349 us
  waiting for transfers between devices  214 us (61%)
  matrix products  50.3 us (14%)
  blocking collectives  32.4 us (9%)
  starting transfers between devices  19.4 us (6%)
  between operations  14.1 us (4%)
  other arithmetic  13.2 us (4%)
  local copies, waits for them, and re-layouts  5.27 us (2%)
    all_gather x1, waiting for transfers between devices, on_device(): all_gate = lax.all_gather(gate_weight[0], 'tp', axis=0)  50.9 us
    dot_general x13, matrix products, f32dot(): return jnp.dot(a, b, preferred_element_type=jnp.float32)  49.8 us
    all_gather x1, waiting for transfers between devices, on_device(): all_up = lax.all_gather(up_weight[0], 'tp', axis=0)  39.8 us
    all_gather x1, waiting for transfers between devices, on_device(): all_down = lax.all_gather(down_weight[0], 'tp', axis=0, tiled=True)  37.1 us
    all_gather x1, waiting for transfers between devices, on_device(): lax.all_gather(arrived, 'ep', axis=0, axis_index_groups=plane_groups, til...  34.6 us
    all_to_all x1, blocking collectives, on_device(): lax.all_to_all(ordered, 'ep', split_axis=0, concat_axis=0, axis_index_gro...  32.4 us
    reduce_scatter x1, waiting for transfers between devices, on_device(): lax.psum_scatter(answers, 'ep', scatter_dimension=0, axis_index_groups=pl...  19 us
    all_to_all x1, waiting for transfers between devices, on_device(): lax.all_to_all(home, 'ep', split_axis=0, concat_axis=0, axis_index_groups...  18.3 us
  transfers between devices with their start and end apart: 9, of which 8 were waited for; matrix products, arithmetic and copies ran while one was open for 13% of the time, Pallas kernels for 0%

profile of v1, /device:TPU:8, one launch (start us, length us, event | category | flops | bytes accessed | tf_op | source)
XLA Modules:
  0.0 348.6 jit_solution(15072283598216035923)
XLA Ops:
  7.2 0.8 fusion.52
  8.0 0.7 and_select_fusion
  8.7 0.7 select_reduce_fusion.1
  9.4 0.7 exponential_reduce_fusion
  10.1 0.7 rev.3
  10.9 0.7 divide_multiply_fusion
  11.8 1.3 fusion.15
  13.2 0.2 convert_reduce_fusion
  13.4 1.3 fusion.17
  14.7 0.3 concatenate.10
  15.0 0.5 convolution_convert_fusion
  15.5 0.1 all_to_all.20
  15.6 32.4 %all_to_all.29 = bf16[8,20,2176]{2,1,0:T(8,128)(2,1)S(1)} all-to-all(bf16[8,20,2176]{2,1,0:T(8,128)(2,1)S(1)} %all_to_all.20), channel_id=1, replica_groups={{0,32,64,96,128,160,192,224},{4,36,68,100,132,164,196,228},{8,40,72,104..., dimensions={0} | all-to-all | bytes 1392640 | tf_op jit(solution)/shard_map/all_to_all | solution.py:75
  48.1 1.0 all_to_all.22
  49.1 0.7 all-gather.8.cloned.1.call-update
  49.9 0.7 all-gather.10.cloned.1.call-update
  50.6 0.5 all-gather.12.cloned.1.call-update
  51.2 34.6 %all-gather.6.cloned.1.call-done = bf16[1280,2176]{1,0:T(8,128)(2,1)} async-done(((bf16[160,2176]{1,0:T(8,128)(2,1)}), bf16[1280,2176]{1,0:T(8,128)(2,1)}) %all-gather.6.cloned.1.call-update) | async-done | bytes 5570576 | tf_op jit(solution)/shard_map/all_gather | solution.py:78
  85.8 1.1 select_reduce_fusion
  87.0 50.9 %all-gather.8.cloned.1.call-done = bf16[4,2048,256]{2,1,0:T(8,128)(2,1)} async-done(((bf16[1,2048,256]{2,1,0:T(8,128)(2,1)}), bf16[4,2048,256]{2,1,0:T(8,128)(2,1)}) %all-gather.8.cloned.1.call-update) | async-done | bytes 4194320 | tf_op jit(solution)/shard_map/all_gather | solution.py:81
  137.9 5.5 %fusion.23 = f32[1280,256]{0,1:T(8,128)} fusion(bf16[4,2048,256]{2,1,0:T(8,128)(2,1)} %all-gather.8.cloned.1.call-done, bf16[1280,2176]{1,0:T(8,128)(2,1)} %all-gather.6.cloned.1.call-done), kind=kOutput, calls=%fused_computation.45 | convolution fusion | flops 1342177280 | bytes 7602176 | tf_op jit(solution)/shard_map/dot_general | solution.py:40
  143.4 0.6 copy-done.5
  144.0 2.7 fusion.22
  146.7 2.7 fusion.21
  149.4 1.6 fusion.20
  151.0 39.8 %all-gather.10.cloned.1.call-done = bf16[4,2048,256]{2,1,0:T(8,128)(2,1)} async-done(((bf16[1,2048,256]{2,1,0:T(8,128)(2,1)}), bf16[4,2048,256]{2,1,0:T(8,128)(2,1)}) %all-gather.10.cloned.1.call-update) | async-done | bytes 4194320 | tf_op jit(solution)/shard_map/all_gather | solution.py:82
  190.8 5.0 %fusion.11 = bf16[1280,256]{0,1:T(8,128)(2,1)S(1)} fusion(f32[1280,256]{0,1:T(8,128)} %fusion.23, bf16[4,2048,256]{2,1,0:T(8,128)(2,1)} %all-gather.10.cloned.1.call-done, bf16[1280,2176]{1,0:T(8,128)(2,1)} %all-gather.6.cloned.1.call-done), kind=kOutput, calls=%fused_computation.20 | convolution fusion | flops 1344143360 | bytes 8257536 | tf_op jit(solution)/shard_map/dot_general | solution.py:40
  195.9 5.2 %fusion.12 = bf16[1280,256]{0,1:T(8,128)(2,1)} fusion(f32[1280,256]{0,1:T(8,128)S(1)} %copy-done.9, bf16[4,2048,256]{2,1,0:T(8,128)(2,1)S(1)} %copy-done.4, bf16[1280,2176]{1,0:T(8,128)(2,1)} %all-gather.6.cloned.1.call-done), kind=kOutput, calls=%fused_computation.21 | convolution fusion | flops 1344143360 | bytes 8257536 | tf_op jit(solution)/shard_map/dot_general | solution.py:40
  201.1 2.6 fusion.13
  203.7 2.8 fusion.14
  206.6 37.1 %all-gather.12.cloned.1.call-done = bf16[1,1024,2048]{2,1,0:T(8,128)(2,1)} async-done(((bf16[1,256,2048]{2,1,0:T(8,128)(2,1)}), bf16[1,1024,2048]{2,1,0:T(8,128)(2,1)}) %all-gather.12.cloned.1.call-update) | async-done | bytes 4194320 | tf_op jit(solution)/shard_map/all_gather | solution.py:83
  243.7 9.9 %multiply_convert_fusion = bf16[1280,2048]{1,0:T(8,128)(2,1)} fusion(f32[1280]{0:T(1024)S(1)} %select_reduce_fusion, bf16[1,1024,2048]{2,1,0:T(8,128)(2,1)} %all-gather.12.cloned.1.call-done, bf16[1280,256]{0,1:T(8,128)(2,1)} %fusion.14, bf16[1280,256]{0,1:T(8,128)(2,1)} %fusion.13, bf16[1280,256]{0,1:T(8,128)(2,1)} %fusion.12, bf16[1280,256]{0,1:T(8,128)(2,1)S(1)} %fusion.11), kind=kOutput, calls=%fused_computation | convolution fusion | flops 5384437760 | bytes 12063744 | tf_op jit(solution)/shard_map/dot_general | solution.py:40
  253.6 2.3 fusion
  256.0 3.1 fusion.46
  259.1 0.9 fusion.19
  260.0 1.6 collective-permute-start
  261.6 1.3 collective-permute-start.1
  262.9 3.2 collective-permute-done.1
  266.1 6.5 %convolution_convert_fusion.1 = bf16[640,2048]{1,0:T(8,128)(2,1)} fusion(bf16[256,2048]{1,0:T(8,128)(2,1)S(1)} %copy-done, bf16[2048,256]{1,0:T(8,128)(2,1)} %param.19, f32[642,256]{1,0:T(8,128)S(1)} %maximum_convert_fusion, f32[256]{0:T(256)S(1)} %bitcast.59, f32[256]{0:T(256)S(1)} %bitcast.60, f32[256]{0:T(256)S(1)} %bitcast.58, ...), kind=kOutput, calls=%fused_computation.8 | convolution fusion | flops 1349877760 | bytes 9321472 | tf_op jit(solution)/shard_map/dot_general | solution.py:40
  272.7 5.7 %all-to-all-start = ((bf16[4,160,2048]{2,1,0:T(8,128)(2,1)}), bf16[4,160,2048]{2,1,0:T(8,128)(2,1)}, u32[]{:S(2)}, u32[]{:S(2)}) async-start(bf16[4,160,2048]{2,1,0:T(8,128)(2,1)} %bitcast.45), calls=%async_computation | async-start | bytes 5242880 | tf_op jit(solution)/shard_map/all_to_all | solution.py:96
  278.4 19.0 %reduce-scatter.2.cloned.1.call-done = bf16[160,2048]{1,0:T(8,128)(2,1)} async-done(((bf16[1280,2048]{1,0:T(8,128)(2,1)}), bf16[160,2048]{1,0:T(8,128)(2,1)}) %reduce-scatter.2.cloned.1.call-update) | async-done | bytes 655376 | tf_op jit(solution)/shard_map/reduce_scatter | solution.py:111
  297.4 2.0 all_to_all.23
  299.4 9.2 %all-to-all-done = bf16[4,160,2048]{2,1,0:T(8,128)(2,1)} async-done(((bf16[4,160,2048]{2,1,0:T(8,128)(2,1)}), bf16[4,160,2048]{2,1,0:T(8,128)(2,1)}, u32[]{:S(2)}, u32[]{:S(2)}) %all-to-all-start) | async-done | bytes 2621472 | tf_op jit(solution)/shard_map/all_to_all | solution.py:96
  308.6 10.7 %all-to-all-start.2 = ((bf16[8,20,2048]{2,1,0:T(8,128)(2,1)}), bf16[8,20,2048]{2,1,0:T(8,128)(2,1)S(1)}, u32[]{:S(2)}, u32[]{:S(2)}) async-start(bf16[8,20,2048]{2,1,0:T(8,128)(2,1)} %all_to_all.23), calls=%async_computation.3 | async-start | bytes 1572864 | tf_op jit(solution)/shard_map/all_to_all | solution.py:114
  319.2 3.3 reduce_sum.69
  322.5 18.3 %all-to-all-done.2 = bf16[8,20,2048]{2,1,0:T(8,128)(2,1)S(1)} async-done(((bf16[8,20,2048]{2,1,0:T(8,128)(2,1)}), bf16[8,20,2048]{2,1,0:T(8,128)(2,1)S(1)}, u32[]{:S(2)}, u32[]{:S(2)}) %all-to-all-start.2) | async-done | bytes 655392 | tf_op jit(solution)/shard_map/all_to_all | solution.py:114
  340.7 0.1 all_to_all.25
  340.9 1.2 convolution_convert_fusion.2
  (47 shorter events, 0.7 us)
Async XLA Ops:
  7.2 259.0 %copy-start = (bf16[256,2048]{1,0:T(8,128)(2,1)S(1)}, bf16[256,2048]{1,0:T(8,128)(2,1)}, u32[]{:S(2)}) copy-start(bf16[256,2048]{1,0:T(8,128)(2,1)} %param.21) | copy-start | bytes 3145732
  7.2 78.6 %all-gather.6.cloned.1.call-start = ((), (), s32[]{:S(2)}) async-start(), calls=%async_computation.4 | async-start | bytes 6266880 | tf_op jit(solution)/shard_map/all_gather | solution.py:78
  49.1 88.8 %all-gather.8.cloned.1.call-start = ((), (), s32[]{:S(2)}) async-start(), calls=%async_computation.5 | async-start | bytes 5242880 | tf_op jit(solution)/shard_map/all_gather | solution.py:81
  49.8 141.0 %all-gather.10.cloned.1.call-start = ((), (), s32[]{:S(2)}) async-start(), calls=%async_computation.6 | async-start | bytes 5242880 | tf_op jit(solution)/shard_map/all_gather | solution.py:82
  50.6 193.1 %all-gather.12.cloned.1.call-start = ((), (), s32[]{:S(2)}) async-start(), calls=%async_computation.8 | async-start | bytes 5242880 | tf_op jit(solution)/shard_map/all_gather | solution.py:83
  51.1 246.2 %reduce-scatter.2.cloned.1.call-start = ((), (), s32[]{:S(2)}) async-start(), calls=%async_computation.7 | async-start | bytes 5898240 | tf_op jit(solution)/shard_map/reduce_scatter | solution.py:111
  137.9 5.6 %copy-start.2 = (bf16[1280,2176]{1,0:T(8,128)(2,1)S(1)}, bf16[1280,2176]{1,0:T(8,128)(2,1)}, u32[]{:S(2)}) copy-start(bf16[1280,2176]{1,0:T(8,128)(2,1)} %all-gather.6.cloned.1.call-done) | copy-start | bytes 16711684
  137.9 6.1 %copy-start.5 = (bf16[4,2048,256]{2,1,0:T(8,128)(2,1)S(1)}, bf16[4,2048,256]{2,1,0:T(8,128)(2,1)}, u32[]{:S(2)}) copy-start(bf16[4,2048,256]{2,1,0:T(8,128)(2,1)} %all-gather.8.cloned.1.call-done) | copy-start | bytes 12582916
  190.8 5.0 %copy-start.4 = (bf16[4,2048,256]{2,1,0:T(8,128)(2,1)S(1)}, bf16[4,2048,256]{2,1,0:T(8,128)(2,1)}, u32[]{:S(2)}) copy-start(bf16[4,2048,256]{2,1,0:T(8,128)(2,1)} %all-gather.10.cloned.1.call-done) | copy-start | bytes 12582916
  190.8 5.0 %copy-start.9 = (f32[1280,256]{0,1:T(8,128)S(1)}, f32[1280,256]{0,1:T(8,128)}, u32[]{:S(2)}) copy-start(f32[1280,256]{0,1:T(8,128)} %fusion.22) | copy-start | bytes 3932164
  190.8 10.3 %slice-start = ((s8[5570560]{0:T(1024)(128)(4,1)}), s8[4194304]{0:T(1024)(128)(4,1)S(1)}, s32[]{:S(2)}) async-start(s8[5570560]{0:T(1024)(128)(4,1)} %bitcast.46), calls=%async_computation.9 | async-start | bytes 8388608
  195.8 5.3 %slice-start.1 = ((s8[5570560]{0:T(1024)(128)(4,1)}), s8[1376256]{0:T(1024)(128)(4,1)S(1)}, s32[]{:S(2)}) async-start(s8[5570560]{0:T(1024)(128)(4,1)} %bitcast.46), calls=%async_computation.10 | async-start | bytes 2752512
  195.9 5.3 %copy-start.8 = (f32[1280,256]{0,1:T(8,128)S(1)}, f32[1280,256]{0,1:T(8,128)}, u32[]{:S(2)}) copy-start(f32[1280,256]{0,1:T(8,128)} %fusion.21) | copy-start | bytes 3932164
  253.6 2.4 copy-start.7
  255.9 3.1 copy-start.1
  256.0 3.1 copy-start.6
  259.1 3.8 %copy-start.3 = (f32[3,256]{1,0:T(4,128)S(1)}, f32[3,256]{1,0:T(4,128)}, u32[]{:S(2)}) copy-start(f32[3,256]{1,0:T(4,128)} %param.20) | copy-start | bytes 9220
  260.0 2.9 collective-permute-start
  261.6 4.5 %collective-permute-start.1 = (bf16[1,256]{1,0:T(2,128)(2,1)S(1)}, bf16[1,256]{1,0:T(2,128)(2,1)S(1)}, u32[]{:S(2)}, u32[]{:S(2)}) collective-permute-start(bf16[1,256]{1,0:T(2,128)(2,1)S(1)} %get-tuple-element.3), channel_id=1, source_target_pairs={{4,0},{8,4},{12,8},{16,12},{20,16},{24,20},{28,24},{32,28},{36,32}... | collective-permute-start | bytes 1544 | tf_op jit(solution)/shard_map/ppermute | solution.py:19
  272.7 35.9 %all-to-all-start = ((bf16[4,160,2048]{2,1,0:T(8,128)(2,1)}), bf16[4,160,2048]{2,1,0:T(8,128)(2,1)}, u32[]{:S(2)}, u32[]{:S(2)}) async-start(bf16[4,160,2048]{2,1,0:T(8,128)(2,1)} %bitcast.45), calls=%async_computation | async-start | bytes 5242880 | tf_op jit(solution)/shard_map/all_to_all | solution.py:96
  308.6 32.2 %all-to-all-start.2 = ((bf16[8,20,2048]{2,1,0:T(8,128)(2,1)}), bf16[8,20,2048]{2,1,0:T(8,128)(2,1)S(1)}, u32[]{:S(2)}, u32[]{:S(2)}) async-start(bf16[8,20,2048]{2,1,0:T(8,128)(2,1)} %all_to_all.23), calls=%async_computation.3 | async-start | bytes 1572864 | tf_op jit(solution)/shard_map/all_to_all | solution.py:114
Sparse Core Ops, SparseCore 0:
  49.2 36.5 all-gather.5
  87.6 50.1 all-gather.7
  139.7 51.1 all-gather.9
  192.5 51.1 all-gather.11
  253.7 43.5 reduce-scatter.1

commit v2 on v1

v2 whole, which is shorter than its diff:
```python
import jax
import jax.numpy as jnp
from jax import lax
from jax.experimental import pallas as pl
from jax.experimental.pallas import tpu as pltpu
from jax.sharding import PartitionSpec as P

MESH = pl.DeviceIdType.MESH
EPSILON = 1e-06
BF16 = jnp.bfloat16
F32 = jnp.float32
D = 2048
WIDE = D + 128
TOK = 160
HALF = 80
PER = 20
PAD = 32
GROUPS = 8
MEMBERS = 8
NX = 4
NY = 4
LOC = 256
CHUNKS = 4
CW = D // CHUNKS
COPIES = 128


def dot(a, b):
    return jnp.dot(a, b, preferred_element_type=F32)


def iota(shape, dim):
    return lax.broadcasted_iota(jnp.int32, shape, dim)


def scaled(wide, gain):
    mean = jnp.mean(wide * wide, axis=-1, keepdims=True)
    return (wide * lax.rsqrt(mean + EPSILON) * gain).astype(BF16)


def kernel(
    mixer_input, mixer_gain, value_weight, inner_gate, outer_gate, taps, mixer_proj,
    expert_input, expert_gain, routes, group_logits, pair_logits, gate_weight, up_weight, down_weight,
    mixer_output, expert_output,
    m_in, w_v, w_i, w_o, w_p, e_in, w_g, w_u, w_d,
    rows, z_out, z_in, tokens, hidden, mixed, outer, m_rows, m_parts, from_prev, from_next,
    m_a, m_b, m_p, m_n,
    parts, pair, r_a, r_b, r_p, r_n, home, zr_out, zr_in, spread, unsort,
    send_sems, recv_sems, local_sems,
):
    ep = lax.axis_index("ep")
    y = lax.axis_index("tp")
    core = lax.rem(ep, 2)
    x = lax.rem(ep // 2, NX)
    z = ep // MEMBERS
    n_ep = GROUPS * MEMBERS

    def at(zz, xx, cc):
        return zz * MEMBERS + xx * 2 + cc

    y_next = (ep, lax.rem(y + 1, NY))
    y_prev = (ep, lax.rem(y + NY - 1, NY))
    x_next = (at(z, lax.rem(x + 1, NX), core), y)
    x_prev = (at(z, lax.rem(x + NX - 1, NX), core), y)
    twin = (at(z, x, 1 - core), y)
    s_next = (lax.rem(ep + 1, n_ep), y)
    s_prev = (lax.rem(ep + n_ep - 1, n_ep), y)
    z_plus = [(at(lax.rem(z + d, GROUPS), x, core), y) for d in range(GROUPS)]
    z_minus = [(at(lax.rem(z + GROUPS - d, GROUPS), x, core), y) for d in range(GROUPS)]

    locals_ = []

    def load(src, dst):
        copy = pltpu.make_async_copy(src, dst, local_sems.at[len(locals_)])
        locals_.append(copy)
        copy.start()
        return copy

    copies = []

    def send(src, dst, device):
        k = len(copies)
        copy = pltpu.make_async_remote_copy(
            src_ref=src, dst_ref=dst, send_sem=send_sems.at[k], recv_sem=recv_sems.at[k],
            device_id=device, device_id_type=MESH,
        )
        copies.append(copy)
        copy.start()
        return copy

    l_ein = load(expert_input, e_in)
    l_min = load(mixer_input, m_in)
    l_v = load(value_weight, w_v)
    l_i = load(inner_gate, w_i)
    l_o = load(outer_gate, w_o)
    l_p = load(mixer_proj, w_p)
    l_g = load(gate_weight.at[0], w_g.at[0])
    l_u = load(up_weight.at[0], w_u.at[0])
    l_d = [
        load(down_weight.at[0, :, pl.ds(k * CW, CW)], w_d.at[k, pl.ds(0, LOC)]) for k in range(CHUNKS)
    ]

    barrier = pltpu.get_barrier_semaphore()
    partners = [y_next, y_prev, x_next, x_prev, twin, s_next, s_prev] + z_plus[1:]
    for device in partners:
        pl.semaphore_signal(barrier, inc=1, device_id=device, device_id_type=MESH)
    pl.semaphore_wait(barrier, len(partners))

    g_next = send(gate_weight.at[0], w_g.at[1], y_next)
    g_prev = send(gate_weight.at[0], w_g.at[3], y_prev)
    u_next = send(up_weight.at[0], w_u.at[1], y_next)
    u_prev = send(up_weight.at[0], w_u.at[3], y_prev)

    l_ein.wait()
    e_gain = expert_gain[...]

    def norm_expert(i, _):
        at_ = pl.ds(pl.multiple_of(i * 32, 32), 32)
        rows[at_, pl.ds(0, D)] = scaled(e_in[at_, :].astype(F32), e_gain)
        return 0

    lax.fori_loop(0, TOK // 32, norm_expert, 0)
    first = routes[:, 0:1]
    second = routes[:, 1:2]
    group = lax.shift_right_logical(first, 3)
    logits = group_logits[...]
    picked = jnp.sum(
        jnp.where(iota((TOK, GROUPS), 1) == group, logits, 0.0), axis=1, keepdims=True
    )
    g_weight = 1.0 / jnp.sum(jnp.exp(logits - picked), axis=1, keepdims=True)
    p0 = pair_logits[:, 0:1]
    p1 = pair_logits[:, 1:2]
    weight0 = g_weight / (1.0 + jnp.exp(p1 - p0))
    weight1 = g_weight / (1.0 + jnp.exp(p0 - p1))
    lane = iota((TOK, 128), 1)
    member = lax.bitwise_and(lane, 7)
    wide_w = jnp.where(member == lax.bitwise_and(first, 7), weight0, 0.0) + jnp.where(
        member == lax.bitwise_and(second, 7), weight1, 0.0
    )
    high = wide_w.astype(BF16).astype(F32)
    extra = jnp.where(lane < 8, high, jnp.where(lane < 16, wide_w - high, 0.0))
    rows[:, pl.ds(D, 128)] = extra.astype(BF16)

    rel = lax.bitwise_and(group + (GROUPS - z), 7).astype(F32)
    square = (TOK, TOK)
    sub, lan = iota(square, 0), iota(square, 1)
    rel_row = jnp.sum(jnp.where(sub == lan, rel, 0.0), axis=0, keepdims=True)
    same = rel == rel_row
    rank_col = jnp.sum(jnp.where(same & (lan < sub), 1.0, 0.0), axis=1, keepdims=True)
    rank_row = jnp.sum(jnp.where(same & (sub < lan), 1.0, 0.0), axis=0, keepdims=True)
    slot_col = (rel * PAD + rank_col).astype(jnp.int32)
    slot_row = (rel_row * PAD + rank_row).astype(jnp.int32)
    unsort[...] = (iota((TOK, GROUPS * PAD), 1) == slot_col).astype(F32).astype(BF16)
    sort = (iota((GROUPS * PAD, TOK), 0) == slot_row).astype(F32).astype(BF16)
    for q in range(4):
        cols = pl.ds(q * CW, CW)
        z_out[:, cols] = dot(sort, rows[:, cols]).astype(BF16)
    z_out[:, pl.ds(D, 128)] = dot(sort, rows[:, pl.ds(D, 128)]).astype(BF16)
    z_sent = [
        send(z_out.at[pl.ds(d * PAD, PAD)], z_in.at[pl.ds(d * PAD, PAD)], z_plus[d])
        for d in range(1, GROUPS)
    ]
    z_in[pl.ds(0, PAD), :] = z_out[pl.ds(0, PAD), :]

    m_gain = mixer_gain[...]
    for copy in (l_min, l_v, l_i, l_o):
        copy.wait()

    def norm_mixer(i, _):
        at_ = pl.ds(pl.multiple_of(i * 32, 32), 32)
        m_in[at_, :] = scaled(m_in[at_, :].astype(F32), m_gain)
        return 0

    lax.fori_loop(0, NY * TOK // 32, norm_mixer, 0)

    def gates(i, _):
        at_ = pl.ds(pl.multiple_of(i * TOK, TOK), TOK)
        block = m_in[at_, :]
        value = dot(block, w_v[...])
        inner = dot(block, w_i[...])
        mixed[pl.ds(pl.multiple_of(i * TOK + 8, 8), TOK), :] = (inner * value).astype(BF16).astype(F32)
        outer[at_, :] = dot(block, w_o[...])
        return 0

    lax.fori_loop(0, NY, gates, 0)
    h_next = send(mixed.at[pl.ds(NY * TOK, 8)], from_prev, s_next)
    h_prev = send(mixed.at[pl.ds(8, 8)], from_next, s_prev)
    l_p.wait()
    h_next.wait_recv()
    h_prev.wait_recv()
    mixed[pl.ds(7, 1), :] = jnp.where(ep == 0, 0.0, from_prev[pl.ds(7, 1), :])
    mixed[pl.ds(NY * TOK + 8, 1), :] = jnp.where(ep == n_ep - 1, 0.0, from_next[pl.ds(0, 1), :])
    t0, t1, t2 = taps[0:1, :], taps[1:2, :], taps[2:3, :]
    for i in range(NY):
        at_ = i * TOK
        conv = (
            t0 * mixed[pl.ds(at_ + 7, TOK), :]
            + t1 * mixed[pl.ds(at_ + 8, TOK), :]
            + t2 * mixed[pl.ds(at_ + 9, TOK), :]
        )
        m_rows[pl.ds(at_, TOK), :] = (outer[pl.ds(at_, TOK), :] * conv).astype(BF16)

    def project(i, _):
        r = i // 4
        cols = pl.ds(pl.multiple_of(lax.rem(i, 4) * CW, CW), CW)
        begin = pl.multiple_of(lax.rem(y + r, NY) * TOK, TOK)
        block = m_rows[pl.ds(begin, TOK), :]
        m_parts[pl.ds(pl.multiple_of(r * TOK, TOK), TOK), cols] = dot(block, w_p[:, cols]).astype(BF16)
        return 0

    lax.fori_loop(0, NY * 4, project, 0)

    g_next.wait_recv()
    f_g = send(w_g.at[1], w_g.at[2], y_next)

    for copy in z_sent:
        copy.wait_recv()
    p_sub = iota((TOK, GROUPS * PAD), 0)
    shift = jnp.zeros((TOK, GROUPS * PAD), jnp.int32)
    for d in range(1, GROUPS):
        shift = shift + jnp.where(p_sub >= d * PER, PAD - PER, 0)
    compact = (iota((TOK, GROUPS * PAD), 1) == p_sub + shift).astype(F32).astype(BF16)
    q_lan = iota((GROUPS * PAD, TOK), 1)
    shift = jnp.zeros((GROUPS * PAD, TOK), jnp.int32)
    for d in range(1, GROUPS):
        shift = shift + jnp.where(q_lan >= d * PER, PAD - PER, 0)
    spread[...] = (iota((GROUPS * PAD, TOK), 0) == q_lan + shift).astype(F32).astype(BF16)
    for q in range(4):
        cols = pl.ds(q * CW, CW)
        tokens[pl.ds(0, TOK), cols] = dot(compact, z_in[:, cols]).astype(BF16)
    tokens[pl.ds(0, TOK), pl.ds(D, 128)] = dot(compact, z_in[:, pl.ds(D, 128)]).astype(BF16)

    def block(b, h=None):
        if h is None:
            return tokens.at[pl.ds(b * TOK, TOK)]
        return tokens.at[pl.ds(b * TOK + h * HALF, HALF)]

    a_next = [None, None]
    a_prev = [None, None]
    a_next[0] = send(block(0, 0), block(1, 0), x_next)
    a_prev[1] = send(block(0, 1), block(3, 1), x_prev)
    a_next[1] = send(block(0, 1), block(1, 1), x_next)
    a_prev[0] = send(block(0, 0), block(3, 0), x_prev)
    c_own = send(block(0), block(4), twin)
    a_next[0].wait_recv()
    f_next = send(block(1, 0), block(2, 0), x_next)
    a_prev[1].wait_recv()
    f_prev = send(block(3, 1), block(2, 1), x_prev)
    a_next[1].wait_recv()
    c_1 = send(block(1), block(5), twin)
    a_prev[0].wait_recv()
    c_3 = send(block(3), block(7), twin)

    u_prev.wait_recv()
    f_u = send(w_u.at[3], w_u.at[2], y_prev)

    d_next = [None] * CHUNKS
    d_prev = [None] * CHUNKS

    def down_send(k):
        src = down_weight.at[0, :, pl.ds(k * CW, CW)]
        d_next[k] = send(src, w_d.at[k, pl.ds(LOC, LOC)], y_next)
        d_prev[k] = send(src, w_d.at[k, pl.ds(3 * LOC, LOC)], y_prev)

    down_send(0)
    down_send(1)

    f_next.wait_recv()
    f_prev.wait_recv()
    c_2 = send(block(2), block(6), twin)
    for copy in (c_own, c_1, c_3, c_2):
        copy.wait_recv()

    TILE = 320
    TILES = MEMBERS * TOK // TILE

    def ffn(j):
        def body(i, _):
            at_ = pl.ds(pl.multiple_of(i * TILE, TILE), TILE)
            block_ = tokens[at_, pl.ds(0, D)]
            a = dot(block_, w_g[j])
            b = dot(block_, w_u[j])
            hidden[at_, pl.ds(j * LOC, LOC)] = (a / (1.0 + jnp.exp(-a)) * b).astype(BF16)
            return 0

        lax.fori_loop(0, TILES, body, 0)

    l_g.wait()
    l_u.wait()
    ffn(0)
    u_next.wait_recv()
    ffn(1)
    g_prev.wait_recv()
    ffn(3)
    f_g.wait_recv()
    f_u.wait_recv()
    ffn(2)
    for copy in l_d:
        copy.wait()

    own = x * 2 + core
    fd_next = [None] * CHUNKS
    fd_prev = [None] * CHUNKS
    e_sent = [None] * CHUNKS
    ra = [None] * CHUNKS
    rb = [None] * CHUNKS
    n_a = [None] * CHUNKS
    n_b = [None] * CHUNKS
    p_a = [None] * CHUNKS
    p_b = [None] * CHUNKS
    z_back = [None] * CHUNKS
    HC = CW // 2

    def down_forward(k):
        d_next[k].wait_recv()
        d_prev[k].wait_recv()
        fd_next[k] = send(
            w_d.at[k, pl.ds(LOC, LOC), pl.ds(0, HC)], w_d.at[k, pl.ds(2 * LOC, LOC), pl.ds(0, HC)], y_next
        )
        fd_prev[k] = send(
            w_d.at[k, pl.ds(3 * LOC, LOC), pl.ds(HC, HC)], w_d.at[k, pl.ds(2 * LOC, LOC), pl.ds(HC, HC)], y_prev
        )

    def results(k):
        fd_next[k].wait_recv()
        fd_prev[k].wait_recv()

        def body(i, _):
            at_ = pl.ds(pl.multiple_of(i * TILE, TILE), TILE)
            both = tokens[at_, pl.ds(D, 128)].astype(F32)
            lane_ = iota((TILE, 128), 1)
            mine = (lane_ == own) | (lane_ == own + 8)
            weight = jnp.sum(jnp.where(mine, both, 0.0), axis=1, keepdims=True)
            parts[k, at_, :] = (dot(hidden[at_, :], w_d[k]) * weight).astype(BF16)
            return 0

        lax.fori_loop(0, TILES, body, 0)
        e_sent[k] = send(parts.at[k, pl.ds(NX * TOK, NX * TOK)], pair.at[k], twin)

    def add_into(ref, k, begin, count, other):
        at_ = pl.ds(begin, count)
        ref[k, at_, :] = (ref[k, at_, :].astype(F32) + other.astype(F32)).astype(BF16)

    def merge(k):
        e_sent[k].wait_recv()
        for rx in (2, 3, 1, 0):
            add_into(parts, k, rx * TOK, TOK, pair[k, pl.ds(rx * TOK, TOK), :])
        rb[k] = send(parts.at[k, pl.ds(2 * TOK + HALF, HALF)], r_b.at[k], x_next)
        ra[k] = send(parts.at[k, pl.ds(2 * TOK, HALF)], r_a.at[k], x_prev)
        n_a[k] = send(parts.at[k, pl.ds(3 * TOK, HALF)], r_p.at[k, pl.ds(0, HALF)], x_next)
        p_b[k] = send(parts.at[k, pl.ds(TOK + HALF, HALF)], r_n.at[k, pl.ds(HALF, HALF)], x_prev)

    def relay(k):
        rb[k].wait_recv()
        add_into(parts, k, 3 * TOK + HALF, HALF, r_b[k])
        n_b[k] = send(parts.at[k, pl.ds(3 * TOK + HALF, HALF)], r_p.at[k, pl.ds(HALF, HALF)], x_next)
        ra[k].wait_recv()
        add_into(parts, k, TOK, HALF, r_a[k])
        p_a[k] = send(parts.at[k, pl.ds(TOK, HALF)], r_n.at[k, pl.ds(0, HALF)], x_prev)

    def arrive(k):
        for copy in (n_a[k], p_b[k], n_b[k], p_a[k]):
            copy.wait_recv()
        total = (
            parts[k, pl.ds(0, TOK), :].astype(F32) + r_p[k].astype(F32) + r_n[k].astype(F32)
        ).astype(BF16)
        zr_out[k] = dot(spread[...], total).astype(BF16)
        z_back[k] = [
            send(zr_out.at[k, pl.ds(d * PAD, PAD)], zr_in.at[k, pl.ds(d * PAD, PAD)], z_minus[d])
            for d in range(1, GROUPS)
        ]
        zr_in[k, pl.ds(0, PAD), :] = zr_out[k, pl.ds(0, PAD), :]

    def finish(k):
        for copy in z_back[k]:
            copy.wait_recv()
        expert_output[:, pl.ds(k * CW, CW)] = dot(unsort[...], zr_in[k]).astype(BF16)

    def m_add(begin, other):
        def body(i, _):
            cols = pl.ds(pl.multiple_of(i * CW, CW), CW)
            at_ = pl.ds(begin, HALF)
            m_parts[at_, cols] = (m_parts[at_, cols].astype(F32) + other[:, cols].astype(F32)).astype(BF16)
            return 0

        lax.fori_loop(0, 4, body, 0)

    down_forward(0)
    down_send(2)
    down_forward(1)
    down_send(3)
    results(0)
    down_forward(2)
    merge(0)
    results(1)
    relay(0)
    merge(1)
    down_forward(3)
    mb = send(m_parts.at[pl.ds(2 * TOK + HALF, HALF)], m_b, y_next)
    ma = send(m_parts.at[pl.ds(2 * TOK, HALF)], m_a, y_prev)
    mn_a = send(m_parts.at[pl.ds(TOK, HALF)], m_p.at[pl.ds(0, HALF)], y_next)
    mp_b = send(m_parts.at[pl.ds(3 * TOK + HALF, HALF)], m_n.at[pl.ds(HALF, HALF)], y_prev)
    arrive(0)
    relay(1)
    results(2)
    arrive(1)
    results(3)
    merge(2)
    merge(3)
    finish(0)
    relay(2)
    relay(3)
    mb.wait_recv()
    m_add(TOK + HALF, m_b)
    mn_b = send(m_parts.at[pl.ds(TOK + HALF, HALF)], m_p.at[pl.ds(HALF, HALF)], y_next)
    ma.wait_recv()
    m_add(3 * TOK, m_a)
    mp_a = send(m_parts.at[pl.ds(3 * TOK, HALF)], m_n.at[pl.ds(0, HALF)], y_prev)
    arrive(2)
    arrive(3)
    finish(1)
    finish(2)
    finish(3)
    for copy in (mn_a, mp_b, mn_b, mp_a):
        copy.wait_recv()

    def m_final(i, _):
        cols = pl.ds(pl.multiple_of(i * CW, CW), CW)
        mixer_output[:, cols] = (
            m_parts[pl.ds(0, TOK), cols].astype(F32) + m_p[:, cols].astype(F32) + m_n[:, cols].astype(F32)
        ).astype(BF16)
        return 0

    lax.fori_loop(0, 4, m_final, 0)
    for copy in copies:
        copy.wait_send()


def on_device(*args):
    args = list(args)
    args[1] = args[1].reshape(1, D)
    args[8] = args[8].reshape(1, D)
    any_ = pl.BlockSpec(memory_space=pl.ANY)
    vmem = pl.BlockSpec(memory_space=pltpu.VMEM)
    big = (0, 2, 3, 4, 6, 7, 12, 13, 14)
    out = jax.ShapeDtypeStruct((TOK, D), BF16)
    rows = MEMBERS * TOK
    scratch = [
        pltpu.VMEM((NY * TOK, D), BF16),
        pltpu.VMEM((D, LOC), BF16),
        pltpu.VMEM((D, LOC), BF16),
        pltpu.VMEM((D, LOC), BF16),
        pltpu.VMEM((LOC, D), BF16),
        pltpu.VMEM((TOK, D), BF16),
        pltpu.VMEM((NY, D, LOC), BF16),
        pltpu.VMEM((NY, D, LOC), BF16),
        pltpu.VMEM((CHUNKS, NY * LOC, CW), BF16),
        pltpu.VMEM((TOK, WIDE), BF16),
        pltpu.VMEM((GROUPS * PAD, WIDE), BF16),
        pltpu.VMEM((GROUPS * PAD, WIDE), BF16),
        pltpu.VMEM((rows, WIDE), BF16),
        pltpu.VMEM((rows, NY * LOC), BF16),
        pltpu.VMEM((NY * TOK + 16, LOC), F32),
        pltpu.VMEM((NY * TOK, LOC), F32),
        pltpu.VMEM((NY * TOK, LOC), BF16),
        pltpu.VMEM((NY * TOK, D), BF16),
        pltpu.VMEM((8, LOC), F32),
        pltpu.VMEM((8, LOC), F32),
        pltpu.VMEM((HALF, D), BF16),
        pltpu.VMEM((HALF, D), BF16),
        pltpu.VMEM((TOK, D), BF16),
        pltpu.VMEM((TOK, D), BF16),
        pltpu.VMEM((CHUNKS, rows, CW), BF16),
        pltpu.VMEM((CHUNKS, NX * TOK, CW), BF16),
        pltpu.VMEM((CHUNKS, HALF, CW), BF16),
        pltpu.VMEM((CHUNKS, HALF, CW), BF16),
        pltpu.VMEM((CHUNKS, TOK, CW), BF16),
        pltpu.VMEM((CHUNKS, TOK, CW), BF16),
        pltpu.VMEM((8, 128), F32),
        pltpu.VMEM((CHUNKS, GROUPS * PAD, CW), BF16),
        pltpu.VMEM((CHUNKS, GROUPS * PAD, CW), BF16),
        pltpu.VMEM((GROUPS * PAD, TOK), BF16),
        pltpu.VMEM((TOK, GROUPS * PAD), BF16),
        pltpu.SemaphoreType.DMA((COPIES,)),
        pltpu.SemaphoreType.DMA((COPIES,)),
        pltpu.SemaphoreType.DMA((16,)),
    ]
    return pl.pallas_call(
        kernel,
        out_shape=(out, out),
        in_specs=[any_ if k in big else vmem for k in range(15)],
        out_specs=(vmem, vmem),
        scratch_shapes=scratch,
        compiler_params=pltpu.CompilerParams(
            collective_id=0, has_side_effects=True, vmem_limit_bytes=67043328
        ),
        name="mixer_and_experts",
    )(*args)


def solution(mesh):
    in_specs = (
        P("ep", None), P(), P(None, "tp"), P(None, "tp"), P(None, "tp"), P(None, "tp"), P("tp", None),
        P(("ep", "tp"), None), P(), P(("ep", "tp"), None), P(("ep", "tp"), None), P(("ep", "tp"), None),
        P("ep", None, "tp"), P("ep", None, "tp"), P("ep", "tp", None),
    )
    out_specs = (P(("ep", "tp"), None), P(("ep", "tp"), None))
    return jax.shard_map(
        on_device, mesh=mesh, in_specs=in_specs, out_specs=out_specs, check_vma=False
    )
```

time: 351 us -> 158 us (0.45)
  waiting for transfers between devices: 214 us -> 0 us
  Pallas kernels: 0 us -> 148 us
  matrix products: 50.3 us -> 0 us
  blocking collectives: 32.4 us -> 0 us
  starting transfers between devices: 19.4 us -> 0 us
  between operations: 14.1 us -> 0.64 us
  other arithmetic: 13.2 us -> 0 us
    all_gather x4 -> x0, waiting for transfers between devices: 162 us -> none  [the longest x1 50.9 us: on_device(): all_gate = lax.all_gather(gate_weight[0], 'tp', axis=0)]
    pallas_call x0 -> x1, Pallas kernels: none -> 148 us  [on_device(): pl.pallas_call(kernel, out_shape=(out, out), in_specs=[any_ if k in big e...]
    dot_general x14 -> x0, matrix products: 50.3 us -> none  [the longest x13 49.8 us: f32dot(): return jnp.dot(a, b, preferred_element_type=jnp.float32)]
    all_to_all x1 -> x0, blocking collectives: 32.4 us -> none  [on_device(): lax.all_to_all(ordered, 'ep', split_axis=0, concat_axis=0, axis_index_gro...]
    all_to_all x2 -> x0, waiting for transfers between devices: 27.4 us -> none  [the longest x1 18.3 us: on_device(): lax.all_to_all(home, 'ep', split_axis=0, concat_axis=0, axis_index_groups...]
    reduce_scatter x1 -> x0, waiting for transfers between devices: 19 us -> none  [on_device(): lax.psum_scatter(answers, 'ep', scatter_dimension=0, axis_index_groups=pl...]
    all_to_all x2 -> x0, starting transfers between devices: 16.3 us -> none  [the longest x1 10.7 us: on_device(): lax.all_to_all(home, 'ep', split_axis=0, concat_axis=0, axis_index_groups...]
    reduce_sum x7 -> x0, other arithmetic: 9.66 us -> none  [the longest x2 3.63 us: normed(): scale = lax.rsqrt(jnp.mean(wide * wide, axis=-1, keepdims=True) + EPSILON)]
  transfers between devices with their start and end apart: 9 -> 0, of which waited for: 8 -> 0; matrix products, arithmetic and copies ran while one was open for 13% -> 0% of each run, Pallas kernels for 0% -> 0%
where the time goes in v2:
time: 158 us; the launch traced here: 157 us
  Pallas kernels  148 us (94%)
  local copies, waits for them, and re-layouts  8.25 us (5%)
    pallas_call x1, Pallas kernels, on_device(): pl.pallas_call(kernel, out_shape=(out, out), in_specs=[any_ if k in big e...  148 us
    unnamed x5, local copies, waits for them, and re-layouts  8.25 us

profile of v2, /device:TPU:8, one launch (start us, length us, event | category | flops | bytes accessed | tf_op | source)
XLA Modules:
  0.0 156.7 jit_solution(8577542626585118278)
XLA Ops:
  0.6 1.4 copy.17.routes
  2.1 1.4 copy.18.group_logits
  3.5 1.4 copy.19.pair_logits
  4.9 147.8 %mixer_and_experts.1 = (bf16[160,2048]{1,0:T(8,128)(2,1)}, bf16[160,2048]{1,0:T(8,128)(2,1)}) custom-call(bf16[640,2048]{1,0:T(8,128)(2,1)} %mixer_input.1, f32[1,2048]{1,0:T(1,128)} %bitcast.2, bf16[2048,256]{1,0:T(8,128)(2,1)} %value_weight.1, bf16[2048,256]{1,0:T(8,128)(2,1)} %inner_gate.1, bf16[2048,256]{1,0:T(8,128)(2,1)} %outer_gate.1, f32[3,256]{1,0:T(4,128)} %taps.1, ...), custom_call_target="tpu_custom_call" | custom-call | tf_op jit(solution)/shard_map/mixer_and_experts/pallas_call | solution.py:488
  152.7 2.0 %copy.22 = bf16[160,2048]{1,0:T(8,128)(2,1)} copy(bf16[160,2048]{1,0:T(8,128)(2,1)} %get-tuple-element.4) | data formatting | bytes 1310720
  154.7 2.0 %copy.23 = bf16[160,2048]{1,0:T(8,128)(2,1)} copy(bf16[160,2048]{1,0:T(8,128)(2,1)} %get-tuple-element.5) | data formatting | bytes 1310720

commit v3 on v2

--- a/solution.py
+++ b/solution.py
@@ -45,7 +45,7 @@
     m_in, w_v, w_i, w_o, w_p, e_in, w_g, w_u, w_d,
     rows, z_out, z_in, tokens, hidden, mixed, outer, m_rows, m_parts, from_prev, from_next,
     m_a, m_b, m_p, m_n,
-    parts, pair, r_a, r_b, r_p, r_n, home, zr_out, zr_in, spread, unsort,
+    parts, pair, r_a, r_b, r_p, r_n, zr_out, zr_in, spread, unsort,
     send_sems, recv_sems, local_sems,
 ):
     ep = lax.axis_index("ep")
@@ -111,6 +111,30 @@
     u_next = send(up_weight.at[0], w_u.at[1], y_next)
     u_prev = send(up_weight.at[0], w_u.at[3], y_prev)
 
+    d_next = [None] * CHUNKS
+    d_prev = [None] * CHUNKS
+
+    def down_send(k):
+        src = down_weight.at[0, :, pl.ds(k * CW, CW)]
+        d_next[k] = send(src, w_d.at[k, pl.ds(LOC, LOC)], y_next)
+        d_prev[k] = send(src, w_d.at[k, pl.ds(3 * LOC, LOC)], y_prev)
+
+    down_send(0)
+
+    fd_next = [None] * CHUNKS
+    fd_prev = [None] * CHUNKS
+    HC = CW // 2
+
+    def down_forward(k):
+        d_next[k].wait_recv()
+        d_prev[k].wait_recv()
+        fd_next[k] = send(
+            w_d.at[k, pl.ds(LOC, LOC), pl.ds(0, HC)], w_d.at[k, pl.ds(2 * LOC, LOC), pl.ds(0, HC)], y_next
+        )
+        fd_prev[k] = send(
+            w_d.at[k, pl.ds(3 * LOC, LOC), pl.ds(HC, HC)], w_d.at[k, pl.ds(2 * LOC, LOC), pl.ds(HC, HC)], y_prev
+        )
+
     l_ein.wait()
     e_gain = expert_gain[...]
 
@@ -120,47 +144,45 @@
         return 0
 
     lax.fori_loop(0, TOK // 32, norm_expert, 0)
-    first = routes[:, 0:1]
-    second = routes[:, 1:2]
+    first = routes[0:1, :]
+    second = routes[1:2, :]
     group = lax.shift_right_logical(first, 3)
     logits = group_logits[...]
-    picked = jnp.sum(
-        jnp.where(iota((TOK, GROUPS), 1) == group, logits, 0.0), axis=1, keepdims=True
-    )
-    g_weight = 1.0 / jnp.sum(jnp.exp(logits - picked), axis=1, keepdims=True)
-    p0 = pair_logits[:, 0:1]
-    p1 = pair_logits[:, 1:2]
+    picked = jnp.sum(jnp.where(iota((GROUPS, TOK), 0) == group, logits, 0.0), axis=0, keepdims=True)
+    g_weight = 1.0 / jnp.sum(jnp.exp(logits - picked), axis=0, keepdims=True)
+    p0 = pair_logits[0:1, :]
+    p1 = pair_logits[1:2, :]
     weight0 = g_weight / (1.0 + jnp.exp(p1 - p0))
     weight1 = g_weight / (1.0 + jnp.exp(p0 - p1))
-    lane = iota((TOK, 128), 1)
-    member = lax.bitwise_and(lane, 7)
+    line = iota((128, TOK), 0)
+    member = lax.bitwise_and(line, 7)
     wide_w = jnp.where(member == lax.bitwise_and(first, 7), weight0, 0.0) + jnp.where(
         member == lax.bitwise_and(second, 7), weight1, 0.0
     )
     high = wide_w.astype(BF16).astype(F32)
-    extra = jnp.where(lane < 8, high, jnp.where(lane < 16, wide_w - high, 0.0))
-    rows[:, pl.ds(D, 128)] = extra.astype(BF16)
-
-    rel = lax.bitwise_and(group + (GROUPS - z), 7).astype(F32)
+    extra = jnp.where(line < 8, high, jnp.where(line < 16, wide_w - high, 0.0)).astype(BF16)
+
+    rel_row = lax.bitwise_and(group + (GROUPS - z), 7).astype(F32)
     square = (TOK, TOK)
     sub, lan = iota(square, 0), iota(square, 1)
-    rel_row = jnp.sum(jnp.where(sub == lan, rel, 0.0), axis=0, keepdims=True)
-    same = rel == rel_row
-    rank_col = jnp.sum(jnp.where(same & (lan < sub), 1.0, 0.0), axis=1, keepdims=True)
-    rank_row = jnp.sum(jnp.where(same & (sub < lan), 1.0, 0.0), axis=0, keepdims=True)
-    slot_col = (rel * PAD + rank_col).astype(jnp.int32)
-    slot_row = (rel_row * PAD + rank_row).astype(jnp.int32)
-    unsort[...] = (iota((TOK, GROUPS * PAD), 1) == slot_col).astype(F32).astype(BF16)
+    rel_col = jnp.sum(jnp.where(sub == lan, rel_row, 0.0), axis=1, keepdims=True)
+    earlier = (rel_col == rel_row) & (sub < lan)
+    slot_row = rel_row * PAD + jnp.sum(jnp.where(earlier, 1.0, 0.0), axis=0, keepdims=True)
+    slot_col = jnp.sum(jnp.where(sub == lan, slot_row, 0.0), axis=1, keepdims=True).astype(jnp.int32)
+    slot_row = slot_row.astype(jnp.int32)
     sort = (iota((GROUPS * PAD, TOK), 0) == slot_row).astype(F32).astype(BF16)
     for q in range(4):
         cols = pl.ds(q * CW, CW)
         z_out[:, cols] = dot(sort, rows[:, cols]).astype(BF16)
-    z_out[:, pl.ds(D, 128)] = dot(sort, rows[:, pl.ds(D, 128)]).astype(BF16)
+    z_out[:, pl.ds(D, 128)] = lax.dot_general(
+        sort, extra, (((1,), (1,)), ((), ())), preferred_element_type=F32
+    ).astype(BF16)
     z_sent = [
         send(z_out.at[pl.ds(d * PAD, PAD)], z_in.at[pl.ds(d * PAD, PAD)], z_plus[d])
         for d in range(1, GROUPS)
     ]
     z_in[pl.ds(0, PAD), :] = z_out[pl.ds(0, PAD), :]
+    unsort[...] = (iota((TOK, GROUPS * PAD), 1) == slot_col).astype(F32).astype(BF16)
 
     m_gain = mixer_gain[...]
     for copy in (l_min, l_v, l_i, l_o):
@@ -246,24 +268,15 @@
     f_next = send(block(1, 0), block(2, 0), x_next)
     a_prev[1].wait_recv()
     f_prev = send(block(3, 1), block(2, 1), x_prev)
+    u_prev.wait_recv()
+    f_u = send(w_u.at[3], w_u.at[2], y_prev)
+    down_send(1)
+    down_forward(0)
+    down_send(2)
     a_next[1].wait_recv()
     c_1 = send(block(1), block(5), twin)
     a_prev[0].wait_recv()
     c_3 = send(block(3), block(7), twin)
-
-    u_prev.wait_recv()
-    f_u = send(w_u.at[3], w_u.at[2], y_prev)
-
-    d_next = [None] * CHUNKS
-    d_prev = [None] * CHUNKS
-
-    def down_send(k):
-        src = down_weight.at[0, :, pl.ds(k * CW, CW)]
-        d_next[k] = send(src, w_d.at[k, pl.ds(LOC, LOC)], y_next)
-        d_prev[k] = send(src, w_d.at[k, pl.ds(3 * LOC, LOC)], y_prev)
-
-    down_send(0)
-    down_send(1)
 
     f_next.wait_recv()
     f_prev.wait_recv()
@@ -299,8 +312,6 @@
         copy.wait()
 
     own = x * 2 + core
-    fd_next = [None] * CHUNKS
-    fd_prev = [None] * CHUNKS
     e_sent = [None] * CHUNKS
     ra = [None] * CHUNKS
     rb = [None] * CHUNKS
@@ -309,17 +320,6 @@
     p_a = [None] * CHUNKS
     p_b = [None] * CHUNKS
     z_back = [None] * CHUNKS
-    HC = CW // 2
-
-    def down_forward(k):
-        d_next[k].wait_recv()
-        d_prev[k].wait_recv()
-        fd_next[k] = send(
-            w_d.at[k, pl.ds(LOC, LOC), pl.ds(0, HC)], w_d.at[k, pl.ds(2 * LOC, LOC), pl.ds(0, HC)], y_next
-        )
-        fd_prev[k] = send(
-            w_d.at[k, pl.ds(3 * LOC, LOC), pl.ds(HC, HC)], w_d.at[k, pl.ds(2 * LOC, LOC), pl.ds(HC, HC)], y_prev
-        )
 
     def results(k):
         fd_next[k].wait_recv()
@@ -385,8 +385,6 @@
 
         lax.fori_loop(0, 4, body, 0)
 
-    down_forward(0)
-    down_send(2)
     down_forward(1)
     down_send(3)
     results(0)
@@ -436,10 +434,24 @@
         copy.wait_send()
 
 
+def deliver(a, b, a_out, b_out, held, sems):
+    loads = [pltpu.make_async_copy(r, held.at[k], sems.at[k]) for k, r in enumerate((a, b))]
+    stores = [pltpu.make_async_copy(held.at[k], r, sems.at[k + 2]) for k, r in enumerate((a_out, b_out))]
+    for copy in loads:
+        copy.start()
+    for copy, store in zip(loads, stores):
+        copy.wait()
+        store.start()
+    for store in stores:
+        store.wait()
+
+
 def on_device(*args):
     args = list(args)
     args[1] = args[1].reshape(1, D)
     args[8] = args[8].reshape(1, D)
+    for k in (9, 10, 11):
+        args[k] = args[k].T
     any_ = pl.BlockSpec(memory_space=pl.ANY)
     vmem = pl.BlockSpec(memory_space=pltpu.VMEM)
     big = (0, 2, 3, 4, 6, 7, 12, 13, 14)
@@ -455,7 +467,7 @@
         pltpu.VMEM((NY, D, LOC), BF16),
         pltpu.VMEM((NY, D, LOC), BF16),
         pltpu.VMEM((CHUNKS, NY * LOC, CW), BF16),
-        pltpu.VMEM((TOK, WIDE), BF16),
+        pltpu.VMEM((TOK, D), BF16),
         pltpu.VMEM((GROUPS * PAD, WIDE), BF16),
         pltpu.VMEM((GROUPS * PAD, WIDE), BF16),
         pltpu.VMEM((rows, WIDE), BF16),
@@ -476,7 +488,6 @@
         pltpu.VMEM((CHUNKS, HALF, CW), BF16),
         pltpu.VMEM((CHUNKS, TOK, CW), BF16),
         pltpu.VMEM((CHUNKS, TOK, CW), BF16),
-        pltpu.VMEM((8, 128), F32),
         pltpu.VMEM((CHUNKS, GROUPS * PAD, CW), BF16),
         pltpu.VMEM((CHUNKS, GROUPS * PAD, CW), BF16),
         pltpu.VMEM((GROUPS * PAD, TOK), BF16),
@@ -485,7 +496,7 @@
         pltpu.SemaphoreType.DMA((COPIES,)),
         pltpu.SemaphoreType.DMA((16,)),
     ]
-    return pl.pallas_call(
+    results = pl.pallas_call(
         kernel,
         out_shape=(out, out),
         in_specs=[any_ if k in big else vmem for k in range(15)],
@@ -496,6 +507,14 @@
         ),
         name="mixer_and_experts",
     )(*args)
+    return pl.pallas_call(
+        deliver,
+        out_shape=(out, out),
+        in_specs=[any_, any_],
+        out_specs=(any_, any_),
+        scratch_shapes=[pltpu.VMEM((2, TOK, D), BF16), pltpu.SemaphoreType.DMA((4,))],
+        name="deliver",
+    )(*results)
 
 
 def solution(mesh):

time: 158 us -> 151 us (0.956)
  local copies, waits for them, and re-layouts: 8.25 us -> 0 us
    unnamed x5 -> x0, local copies, waits for them, and re-layouts: 8.25 us -> none
    pallas_call x0 -> x1, Pallas kernels: none -> 2.17 us  [on_device(): pl.pallas_call(deliver, out_shape=(out, out), in_specs=[any_, any_], out_...]
    pallas_call x1, Pallas kernels: 148 us -> 146 us  [on_device(): pl.pallas_call(kernel, out_shape=(out, out), in_specs=[any_ if k in big e...]
where the time goes in v3:
time: 151 us; the launch traced here: 149 us
  Pallas kernels  148 us (98%)
    pallas_call x1, Pallas kernels, on_device(): pl.pallas_call(kernel, out_shape=(out, out), in_specs=[any_ if k in big e...  146 us

profile of v3, /device:TPU:8, one launch (start us, length us, event | category | flops | bytes accessed | tf_op | source)
XLA Modules:
  0.0 148.9 jit_solution(9374850994813350631)
XLA Ops:
  0.6 146.1 %mixer_and_experts.1 = (bf16[160,2048]{1,0:T(8,128)(2,1)}, bf16[160,2048]{1,0:T(8,128)(2,1)}) custom-call(bf16[640,2048]{1,0:T(8,128)(2,1)} %mixer_input.1, f32[1,2048]{1,0:T(1,128)} %bitcast.5, bf16[2048,256]{1,0:T(8,128)(2,1)} %value_weight.1, bf16[2048,256]{1,0:T(8,128)(2,1)} %inner_gate.1, bf16[2048,256]{1,0:T(8,128)(2,1)} %outer_gate.1, f32[3,256]{1,0:T(4,128)} %taps.1, ...), custom_call_target="tpu_custom_call" | custom-call | tf_op jit(solution)/shard_map/mixer_and_experts/pallas_call | solution.py:499
  146.8 2.2 %deliver.1 = (bf16[160,2048]{1,0:T(8,128)(2,1)}, bf16[160,2048]{1,0:T(8,128)(2,1)}) custom-call(bf16[160,2048]{1,0:T(8,128)(2,1)} %get-tuple-element.4.a, bf16[160,2048]{1,0:T(8,128)(2,1)} %get-tuple-element.5.b), custom_call_target="tpu_custom_call" | custom-call | tf_op jit(solution)/shard_map/deliver/pallas_call | solution.py:510

commit v4 on v3

--- a/solution.py
+++ b/solution.py
@@ -20,9 +20,15 @@
 NX = 4
 NY = 4
 LOC = 256
-CHUNKS = 4
-CW = D // CHUNKS
-COPIES = 128
+CW = 512
+SIZES = (512, 512, 512, 256, 256)
+CHUNKS = len(SIZES)
+STARTS = tuple(sum(SIZES[:k]) for k in range(CHUNKS))
+COPIES = 160
+
+
+def chunk(k):
+    return pl.ds(STARTS[k], SIZES[k])
 
 
 def dot(a, b):
@@ -96,9 +102,7 @@
     l_p = load(mixer_proj, w_p)
     l_g = load(gate_weight.at[0], w_g.at[0])
     l_u = load(up_weight.at[0], w_u.at[0])
-    l_d = [
-        load(down_weight.at[0, :, pl.ds(k * CW, CW)], w_d.at[k, pl.ds(0, LOC)]) for k in range(CHUNKS)
-    ]
+    l_d = load(down_weight.at[0], w_d.at[pl.ds(0, LOC)])
 
     barrier = pltpu.get_barrier_semaphore()
     partners = [y_next, y_prev, x_next, x_prev, twin, s_next, s_prev] + z_plus[1:]
@@ -115,25 +119,22 @@
     d_prev = [None] * CHUNKS
 
     def down_send(k):
-        src = down_weight.at[0, :, pl.ds(k * CW, CW)]
-        d_next[k] = send(src, w_d.at[k, pl.ds(LOC, LOC)], y_next)
-        d_prev[k] = send(src, w_d.at[k, pl.ds(3 * LOC, LOC)], y_prev)
+        src = down_weight.at[0, :, chunk(k)]
+        d_next[k] = send(src, w_d.at[pl.ds(LOC, LOC), chunk(k)], y_next)
+        d_prev[k] = send(src, w_d.at[pl.ds(3 * LOC, LOC), chunk(k)], y_prev)
 
     down_send(0)
 
     fd_next = [None] * CHUNKS
     fd_prev = [None] * CHUNKS
-    HC = CW // 2
 
     def down_forward(k):
         d_next[k].wait_recv()
         d_prev[k].wait_recv()
-        fd_next[k] = send(
-            w_d.at[k, pl.ds(LOC, LOC), pl.ds(0, HC)], w_d.at[k, pl.ds(2 * LOC, LOC), pl.ds(0, HC)], y_next
-        )
-        fd_prev[k] = send(
-            w_d.at[k, pl.ds(3 * LOC, LOC), pl.ds(HC, HC)], w_d.at[k, pl.ds(2 * LOC, LOC), pl.ds(HC, HC)], y_prev
-        )
+        half = SIZES[k] // 2
+        left, right = pl.ds(STARTS[k], half), pl.ds(STARTS[k] + half, half)
+        fd_next[k] = send(w_d.at[pl.ds(LOC, LOC), left], w_d.at[pl.ds(2 * LOC, LOC), left], y_next)
+        fd_prev[k] = send(w_d.at[pl.ds(3 * LOC, LOC), right], w_d.at[pl.ds(2 * LOC, LOC), right], y_prev)
 
     l_ein.wait()
     e_gain = expert_gain[...]
@@ -308,8 +309,7 @@
     f_g.wait_recv()
     f_u.wait_recv()
     ffn(2)
-    for copy in l_d:
-        copy.wait()
+    l_d.wait()
 
     own = x * 2 + core
     e_sent = [None] * CHUNKS
@@ -331,50 +331,50 @@
             lane_ = iota((TILE, 128), 1)
             mine = (lane_ == own) | (lane_ == own + 8)
             weight = jnp.sum(jnp.where(mine, both, 0.0), axis=1, keepdims=True)
-            parts[k, at_, :] = (dot(hidden[at_, :], w_d[k]) * weight).astype(BF16)
+            parts[at_, chunk(k)] = (dot(hidden[at_, :], w_d[:, chunk(k)]) * weight).astype(BF16)
             return 0
 
         lax.fori_loop(0, TILES, body, 0)
-        e_sent[k] = send(parts.at[k, pl.ds(NX * TOK, NX * TOK)], pair.at[k], twin)
+        e_sent[k] = send(parts.at[pl.ds(NX * TOK, NX * TOK), chunk(k)], pair.at[:, chunk(k)], twin)
 
     def add_into(ref, k, begin, count, other):
         at_ = pl.ds(begin, count)
-        ref[k, at_, :] = (ref[k, at_, :].astype(F32) + other.astype(F32)).astype(BF16)
+        ref[at_, chunk(k)] = (ref[at_, chunk(k)].astype(F32) + other.astype(F32)).astype(BF16)
 
     def merge(k):
         e_sent[k].wait_recv()
         for rx in (2, 3, 1, 0):
-            add_into(parts, k, rx * TOK, TOK, pair[k, pl.ds(rx * TOK, TOK), :])
-        rb[k] = send(parts.at[k, pl.ds(2 * TOK + HALF, HALF)], r_b.at[k], x_next)
-        ra[k] = send(parts.at[k, pl.ds(2 * TOK, HALF)], r_a.at[k], x_prev)
-        n_a[k] = send(parts.at[k, pl.ds(3 * TOK, HALF)], r_p.at[k, pl.ds(0, HALF)], x_next)
-        p_b[k] = send(parts.at[k, pl.ds(TOK + HALF, HALF)], r_n.at[k, pl.ds(HALF, HALF)], x_prev)
+            add_into(parts, k, rx * TOK, TOK, pair[pl.ds(rx * TOK, TOK), chunk(k)])
+        rb[k] = send(parts.at[pl.ds(2 * TOK + HALF, HALF), chunk(k)], r_b.at[:, chunk(k)], x_next)
+        ra[k] = send(parts.at[pl.ds(2 * TOK, HALF), chunk(k)], r_a.at[:, chunk(k)], x_prev)
+        n_a[k] = send(parts.at[pl.ds(3 * TOK, HALF), chunk(k)], r_p.at[pl.ds(0, HALF), chunk(k)], x_next)
+        p_b[k] = send(parts.at[pl.ds(TOK + HALF, HALF), chunk(k)], r_n.at[pl.ds(HALF, HALF), chunk(k)], x_prev)
 
     def relay(k):
         rb[k].wait_recv()
-        add_into(parts, k, 3 * TOK + HALF, HALF, r_b[k])
-        n_b[k] = send(parts.at[k, pl.ds(3 * TOK + HALF, HALF)], r_p.at[k, pl.ds(HALF, HALF)], x_next)
+        add_into(parts, k, 3 * TOK + HALF, HALF, r_b[:, chunk(k)])
+        n_b[k] = send(parts.at[pl.ds(3 * TOK + HALF, HALF), chunk(k)], r_p.at[pl.ds(HALF, HALF), chunk(k)], x_next)
         ra[k].wait_recv()
-        add_into(parts, k, TOK, HALF, r_a[k])
-        p_a[k] = send(parts.at[k, pl.ds(TOK, HALF)], r_n.at[k, pl.ds(0, HALF)], x_prev)
+        add_into(parts, k, TOK, HALF, r_a[:, chunk(k)])
+        p_a[k] = send(parts.at[pl.ds(TOK, HALF), chunk(k)], r_n.at[pl.ds(0, HALF), chunk(k)], x_prev)
 
     def arrive(k):
         for copy in (n_a[k], p_b[k], n_b[k], p_a[k]):
             copy.wait_recv()
         total = (
-            parts[k, pl.ds(0, TOK), :].astype(F32) + r_p[k].astype(F32) + r_n[k].astype(F32)
+            parts[pl.ds(0, TOK), chunk(k)].astype(F32) + r_p[:, chunk(k)].astype(F32) + r_n[:, chunk(k)].astype(F32)
         ).astype(BF16)
-        zr_out[k] = dot(spread[...], total).astype(BF16)
+        zr_out[:, chunk(k)] = dot(spread[...], total).astype(BF16)
         z_back[k] = [
-            send(zr_out.at[k, pl.ds(d * PAD, PAD)], zr_in.at[k, pl.ds(d * PAD, PAD)], z_minus[d])
+            send(zr_out.at[pl.ds(d * PAD, PAD), chunk(k)], zr_in.at[pl.ds(d * PAD, PAD), chunk(k)], z_minus[d])
             for d in range(1, GROUPS)
         ]
-        zr_in[k, pl.ds(0, PAD), :] = zr_out[k, pl.ds(0, PAD), :]
+        zr_in[pl.ds(0, PAD), chunk(k)] = zr_out[pl.ds(0, PAD), chunk(k)]
 
     def finish(k):
         for copy in z_back[k]:
             copy.wait_recv()
-        expert_output[:, pl.ds(k * CW, CW)] = dot(unsort[...], zr_in[k]).astype(BF16)
+        expert_output[:, chunk(k)] = dot(unsort[...], zr_in[:, chunk(k)]).astype(BF16)
 
     def m_add(begin, other):
         def body(i, _):
@@ -388,26 +388,31 @@
     down_forward(1)
     down_send(3)
     results(0)
+    merge(0)
     down_forward(2)
-    merge(0)
+    down_send(4)
     results(1)
     relay(0)
+    down_forward(3)
     merge(1)
-    down_forward(3)
+    results(2)
+    down_forward(4)
     mb = send(m_parts.at[pl.ds(2 * TOK + HALF, HALF)], m_b, y_next)
     ma = send(m_parts.at[pl.ds(2 * TOK, HALF)], m_a, y_prev)
     mn_a = send(m_parts.at[pl.ds(TOK, HALF)], m_p.at[pl.ds(0, HALF)], y_next)
     mp_b = send(m_parts.at[pl.ds(3 * TOK + HALF, HALF)], m_n.at[pl.ds(HALF, HALF)], y_prev)
     arrive(0)
     relay(1)
-    results(2)
+    merge(2)
+    results(3)
+    results(4)
+    merge(3)
+    merge(4)
     arrive(1)
-    results(3)
-    merge(2)
-    merge(3)
-    finish(0)
     relay(2)
     relay(3)
+    relay(4)
+    finish(0)
     mb.wait_recv()
     m_add(TOK + HALF, m_b)
     mn_b = send(m_parts.at[pl.ds(TOK + HALF, HALF)], m_p.at[pl.ds(HALF, HALF)], y_next)
@@ -416,9 +421,9 @@
     mp_a = send(m_parts.at[pl.ds(3 * TOK, HALF)], m_n.at[pl.ds(0, HALF)], y_prev)
     arrive(2)
     arrive(3)
-    finish(1)
-    finish(2)
-    finish(3)
+    arrive(4)
+    for k in range(1, CHUNKS):
+        finish(k)
     for copy in (mn_a, mp_b, mn_b, mp_a):
         copy.wait_recv()
 
@@ -466,7 +471,7 @@
         pltpu.VMEM((TOK, D), BF16),
         pltpu.VMEM((NY, D, LOC), BF16),
         pltpu.VMEM((NY, D, LOC), BF16),
-        pltpu.VMEM((CHUNKS, NY * LOC, CW), BF16),
+        pltpu.VMEM((NY * LOC, D), BF16),
         pltpu.VMEM((TOK, D), BF16),
         pltpu.VMEM((GROUPS * PAD, WIDE), BF16),
         pltpu.VMEM((GROUPS * PAD, WIDE), BF16),
@@ -482,14 +487,14 @@
         pltpu.VMEM((HALF, D), BF16),
         pltpu.VMEM((TOK, D), BF16),
         pltpu.VMEM((TOK, D), BF16),
-        pltpu.VMEM((CHUNKS, rows, CW), BF16),
-        pltpu.VMEM((CHUNKS, NX * TOK, CW), BF16),
-        pltpu.VMEM((CHUNKS, HALF, CW), BF16),
-        pltpu.VMEM((CHUNKS, HALF, CW), BF16),
-        pltpu.VMEM((CHUNKS, TOK, CW), BF16),
-        pltpu.VMEM((CHUNKS, TOK, CW), BF16),
-        pltpu.VMEM((CHUNKS, GROUPS * PAD, CW), BF16),
-        pltpu.VMEM((CHUNKS, GROUPS * PAD, CW), BF16),
+        pltpu.VMEM((rows, D), BF16),
+        pltpu.VMEM((NX * TOK, D), BF16),
+        pltpu.VMEM((HALF, D), BF16),
+        pltpu.VMEM((HALF, D), BF16),
+        pltpu.VMEM((TOK, D), BF16),
+        pltpu.VMEM((TOK, D), BF16),
+        pltpu.VMEM((GROUPS * PAD, D), BF16),
+        pltpu.VMEM((GROUPS * PAD, D), BF16),
         pltpu.VMEM((GROUPS * PAD, TOK), BF16),
         pltpu.VMEM((TOK, GROUPS * PAD), BF16),
         pltpu.SemaphoreType.DMA((COPIES,)),

time: 151 us -> 146 us (0.967); the launches traced: 149 us -> 146 us
  Pallas kernels: 148 us -> 145 us
    pallas_call x1, Pallas kernels: 146 us -> 143 us  [on_device(): pl.pallas_call(kernel, out_shape=(out, out), in_specs=[any_ if k in big e...]
where the time goes in v4:
time: 146 us
  Pallas kernels  145 us (99%)
    pallas_call x1, Pallas kernels, on_device(): pl.pallas_call(kernel, out_shape=(out, out), in_specs=[any_ if k in big e...  143 us

profile of v4, /device:TPU:8, one launch (start us, length us, event | category | flops | bytes accessed | tf_op | source)
XLA Modules:
  0.0 146.0 jit_solution(15936703049702148152)
XLA Ops:
  0.6 143.2 %mixer_and_experts.1 = (bf16[160,2048]{1,0:T(8,128)(2,1)}, bf16[160,2048]{1,0:T(8,128)(2,1)}) custom-call(bf16[640,2048]{1,0:T(8,128)(2,1)} %mixer_input.1, f32[1,2048]{1,0:T(1,128)} %bitcast.5, bf16[2048,256]{1,0:T(8,128)(2,1)} %value_weight.1, bf16[2048,256]{1,0:T(8,128)(2,1)} %inner_gate.1, bf16[2048,256]{1,0:T(8,128)(2,1)} %outer_gate.1, f32[3,256]{1,0:T(4,128)} %taps.1, ...), custom_call_target="tpu_custom_call" | custom-call | tf_op jit(solution)/shard_map/mixer_and_experts/pallas_call | solution.py:504
  143.8 2.2 %deliver.1 = (bf16[160,2048]{1,0:T(8,128)(2,1)}, bf16[160,2048]{1,0:T(8,128)(2,1)}) custom-call(bf16[160,2048]{1,0:T(8,128)(2,1)} %get-tuple-element.4.a, bf16[160,2048]{1,0:T(8,128)(2,1)} %get-tuple-element.5.b), custom_call_target="tpu_custom_call" | custom-call | tf_op jit(solution)/shard_map/deliver/pallas_call | solution.py:515
